TPU v7x, 128 devices: a whole 4x4x4 slice. The times are simulated.
128 devices in a mesh: sp: 16 (over z, y), dp: 8 (over x, core).
Axes of the slice: x: 4, y: 4, z: 4, core: 2. Of those that a mesh axis runs over, the one named last changes fastest.
Arguments:
- residual: bfloat16 [8, 2048, 2048], P('dp', 'sp'), may hold values from -6 to 6
- query_maps: bfloat16 [8, 2048, 2048], P('dp', 'sp'), may hold values from -200 to 200
- key_maps: bfloat16 [8, 2048, 2048], P('dp', 'sp'), may hold values from -200 to 200
- value_rows: bfloat16 [8, 2048, 2048], P('dp', 'sp'), may hold values from -6 to 6
- lambdas: float32 [16], replicated, may hold values from 0.3 to 0.8
- head_gain: float32 [2048], replicated, may hold values from 0.1 to 1.9
- out_weight: bfloat16 [2048, 2048], replicated, may hold values from -0.125 to 0.125
- ffn_gain: float32 [2048], replicated, may hold values from 0.1 to 1.9
- routes: int32 [8, 2048, 2], P('dp', 'sp'), may hold values from 0 to 127, all different within a row; in each aligned block of 128 rows (0 to 127, 128 to 255, ..., all dimensions but the last counted through in order) at most 4 rows name the same one
- route_weights: float32 [8, 2048, 2], P('dp', 'sp'), may hold values from 0.2 to 1
- expert_gate: bfloat16 [128, 2048, 1024], P(('sp', 'dp')), may hold values from -0.125 to 0.125
- expert_up: bfloat16 [128, 2048, 1024], P(('sp', 'dp')), may hold values from -0.125 to 0.125
- expert_down: bfloat16 [128, 1024, 2048], P(('sp', 'dp')), may hold values from -0.1875 to 0.1875
Outputs:
- layer_out: bfloat16 [8, 2048, 2048], P('dp', 'sp')
Inputs may be any that keep to these rules, and one draw needn't show every extreme that they name: `routes`: A token's 2 experts differ; among the 128 rows of one device no expert is named more than 4 times, and in every draw some expert is named exactly 4 times by one device's rows.
All inputs are finite; a program needn't handle non-finite values.
Results may differ from a plain program's by a relative error of at most 0.012.
Values may be sent and summed in bfloat16 or wider, within the bound.
A program may use at most 128 MiB of HBM per device.

v0:
```python
import jax
import jax.numpy as jnp
from jax import lax
from jax.sharding import Mesh
from jax.sharding import PartitionSpec as P

D = 2048
HEADS = 16
HD = 64
VD = 128
SP = ("sp_0", "sp_1")
SP_DP = ("sp_0", "sp_1", "dp")


eps = 1e-06


def side_by_side(arrays, axis, split_dim, concat_dim, along):
    both = jnp.concatenate(arrays, axis=along)
    whole, at, finished = (
        lax.all_to_all(both, axis, split_axis=split_dim, concat_axis=concat_dim, tiled=True),
        0,
        [],
    )
    for a in arrays:
        finished.append(lax.slice_in_dim(whole, at, at + a.shape[along], axis=along))
        at += a.shape[along]
    return tuple(finished)


def in_blocks(value, dim, size):
    lengths = value.shape
    blocks = value.reshape(*lengths[:dim], size, lengths[dim] // size, *lengths[dim + 1 :])
    return jnp.moveaxis(blocks, dim, 0)


def laid_out(blocks, dim):
    blocks = jnp.moveaxis(blocks, 0, dim)
    lengths = blocks.shape
    return blocks.reshape(*lengths[:dim], lengths[dim] * lengths[dim + 1], *lengths[dim + 2 :])


def exchange_in_order(blocks, axes, sequence):
    lengths = [lax.axis_size(a) for a in axes]
    blocks = blocks.reshape(*lengths, *blocks.shape[1:])
    for k in sequence:
        blocks = lax.all_to_all(blocks, axes[k], split_axis=k, concat_axis=k, tiled=True)
    return blocks.reshape(-1, *blocks.shape[len(axes) :])


def one_axis_at_a_time(value, axes, sequence, split_dim, concat_dim):
    blocks = in_blocks(value, split_dim, lax.axis_size(axes))
    return laid_out(exchange_in_order(blocks, axes, sequence), concat_dim)


def exchange_both(value, axis, axes, splits, concats):
    sizes = [lax.axis_size(a) for a in axes]
    blocks = in_blocks(value, splits[0], sizes[0])
    blocks = jnp.moveaxis(in_blocks(blocks, splits[1] + 1, sizes[1]), 0, 1)
    inside = blocks.shape[2:]
    blocks = blocks.reshape(-1, *inside)
    blocks = lax.all_to_all(blocks, axis, split_axis=0, concat_axis=0, tiled=True)
    blocks = laid_out(blocks.reshape(*sizes, *inside), concats[0] + 1)
    return laid_out(blocks, concats[1])


def attend_head(query_head, key_head, value_head, lam_head, gain_head):
    length = query_head.shape[0]
    block_rows = min(512, length)
    count_blocks = length // block_rows
    scaling = query_head.shape[-1] ** (-0.5)
    query_blocks = query_head.reshape(count_blocks, block_rows, 2, query_head.shape[-1])

    def one_block(query_block):
        scores = (
            jnp.einsum("qmd,kmd->mqk", query_block, key_head, preferred_element_type=jnp.float32)
            * scaling
        )
        probabilities = jax.nn.softmax(scores, axis=-1)
        mixed_map = (probabilities[0] - lam_head * probabilities[1]).astype(jnp.bfloat16)
        head_out = jnp.dot(mixed_map, value_head, preferred_element_type=jnp.float32)
        normed = head_out * lax.rsqrt(jnp.mean(head_out * head_out, axis=-1, keepdims=True) + eps)
        return (normed * gain_head * 0.8).astype(jnp.bfloat16)

    return lax.map(one_block, query_blocks).reshape(length, value_head.shape[-1])


def on_device(
    residual,
    query_maps,
    key_maps,
    value_rows,
    lambdas,
    head_gain,
    out_weight,
    ffn_gain,
    routes,
    route_weights,
    expert_gate,
    expert_up,
    expert_down,
):
    count_sp = lax.axis_size(SP)
    count_dp = lax.axis_size("dp")
    heads_here = HEADS // count_sp
    queries, keys_all, values_all = side_by_side((query_maps, key_maps, value_rows), SP, 2, 1, 0)
    first_head = lax.axis_index(SP) * heads_here
    lam_here = lax.dynamic_slice_in_dim(lambdas, first_head, heads_here)
    gain_here = lax.dynamic_slice_in_dim(head_gain, first_head * VD, heads_here * VD)
    query_head = queries[0, :, 0 : 2 * HD].reshape(-1, 2, HD)
    key_head = keys_all[0, :, 0 : 2 * HD].reshape(-1, 2, HD)
    value_head = values_all[0, :, 0:VD]
    outputs = attend_head(query_head, key_head, value_head, lam_here[0], gain_here)
    attended = outputs[None]
    returned_heads = one_axis_at_a_time(attended, SP, (0, 1), 1, 2)
    projected = jnp.dot(returned_heads[0], out_weight, preferred_element_type=jnp.float32)
    residual_mid = (residual[0].astype(jnp.float32) + projected).astype(jnp.bfloat16)
    middle = residual_mid.astype(jnp.float32)
    expert_input = (
        middle * lax.rsqrt(jnp.mean(middle * middle, axis=-1, keepdims=True) + eps) * ffn_gain
    ).astype(jnp.bfloat16)
    tok_rows = residual.shape[1]
    experts_all = count_sp * count_dp
    capacity = max(2, 4 * tok_rows // experts_all)
    flat_routes = routes[0].reshape(-1)
    flat_weights = route_weights[0].reshape(-1)
    onehot = (flat_routes[:, None] == jnp.arange(experts_all, dtype=jnp.int32)[None, :]).astype(
        jnp.int32
    )
    before = jnp.cumsum(onehot, axis=0) - onehot
    rank_of = jnp.sum(before * onehot, axis=1)
    slot = flat_routes * capacity + rank_of
    token_of = jnp.arange(flat_routes.shape[0], dtype=jnp.int32) // routes.shape[2]
    slot_token = jnp.full((experts_all * capacity,), tok_rows, jnp.int32).at[slot].set(token_of)
    padded_input = jnp.concatenate([expert_input, jnp.zeros((1, D), jnp.bfloat16)], axis=0)
    buffer = padded_input[slot_token].reshape(experts_all, capacity, D)
    shaped = buffer.reshape(count_sp, count_dp, capacity, D)
    received = exchange_both(shaped, SP_DP, (SP, "dp"), (0, 1), (0, 1))
    row_block = received.reshape(-1, D)
    gate_part = jnp.dot(row_block, expert_gate[0], preferred_element_type=jnp.float32)
    up_part = jnp.dot(row_block, expert_up[0], preferred_element_type=jnp.float32)
    hidden = (jax.nn.silu(gate_part) * up_part).astype(jnp.bfloat16)
    expert_out = jnp.dot(hidden, expert_down[0], preferred_element_type=jnp.float32).astype(
        jnp.bfloat16
    )
    returned = exchange_both(expert_out.reshape(received.shape), SP_DP, (SP, "dp"), (0, 1), (0, 1))
    picked = returned.reshape(experts_all * capacity, D)[slot]
    weighted = (picked.astype(jnp.float32) * flat_weights[:, None]).reshape(
        tok_rows, routes.shape[2], D
    )
    layer_out = (middle + jnp.sum(weighted, axis=1)).astype(jnp.bfloat16)
    return layer_out[None]


def solution(mesh):
    finer = Mesh(mesh.devices.reshape(4, 4, mesh.shape["dp"]), ("sp_0", "sp_1", "dp"))
    placed = (
        P("dp", SP, None),
        P("dp", SP, None),
        P("dp", SP, None),
        P("dp", SP, None),
        P(),
        P(),
        P(),
        P(),
        P("dp", SP, None),
        P("dp", SP, None),
        P(SP_DP, None, None),
        P(SP_DP, None, None),
        P(SP_DP, None, None),
    )
    return jax.shard_map(
        on_device, mesh=finer, in_specs=placed, out_specs=P("dp", SP, None), check_vma=False
    )
```

profile of v0, /device:TPU:1, one launch (start us, length us, event | category | flops | bytes accessed | tf_op | source)
XLA Modules:
  0.0 236.5 jit_solution(16447463761068725276)
XLA Ops:
  0.0 1.5 pad_maximum_fusion
  1.5 2.5 %copy.46 = bf16[3,128,2048]{1,0,2:T(4,128)(2,1)} copy(bf16[3,128,2048]{2,1,0:T(8,128)(2,1)S(1)} %pad_maximum_fusion) | data formatting | bytes 3145728 | tf_op jit(solution)/shard_map/concatenate | solution.py:19
  4.1 8.7 %all-to-all-start = ((bf16[3,128,2048]{1,0,2:T(4,128)(2,1)}), bf16[3,128,2048]{1,0,2:T(4,128)(2,1)S(1)}, u32[]{:S(2)}, u32[]{:S(2)}) async-start(bf16[3,128,2048]{1,0,2:T(4,128)(2,1)} %copy.46), calls=%async_computation | async-start | bytes 4194304 | tf_op jit(solution)/shard_map/all_to_all | solution.py:21
  12.8 0.1 copy.55
  12.9 0.1 eq.29
  13.1 0.1 copy.57
  13.2 0.2 fusion.45
  13.5 0.8 dynamic_slice.11
  14.2 0.6 dynamic_slice.10
  14.8 29.0 %all-to-all-done = bf16[3,128,2048]{1,0,2:T(4,128)(2,1)S(1)} async-done(((bf16[3,128,2048]{1,0,2:T(4,128)(2,1)}), bf16[3,128,2048]{1,0,2:T(4,128)(2,1)S(1)}, u32[]{:S(2)}, u32[]{:S(2)}) %all-to-all-start) | async-done | bytes 1572896 | tf_op jit(solution)/shard_map/all_to_all | solution.py:21
  43.8 1.3 copy.66
  45.1 0.3 fusion.58
  45.3 0.2 reshape_reshape_squeeze.3
  45.6 0.5 copy.48
  46.1 0.2 reshape_squeeze.4
  46.3 46.7 %while.10 = (s32[]{:T(128)}, bf16[4,512,128]{2,1,0:T(8,128)(2,1)}, bf16[4,512,2,64]{1,3,2,0:T(8,128)(2,1)S(1)}, bf16[2048,2,64]{0,2,1:T(8,128)(2,1)S(1)}, f32[]{...) while((s32[]{:T(128)}, bf16[4,512,128]{2,1,0:T(8,128)(2,1)}, ...), condition=%wide.region_4.5_spmd, body=%wide.region_0.4_spmd.sunk | while | flops 548801024 | bytes 35931228 | solution.py:85
  46.4 4.9 %fusion.74 = (f32[2,512]{1,0:T(2,128)S(1)}, f32[2,512,2048]{2,1,0:T(8,128)}) fusion(bf16[2048,2,64]{0,2,1:T(8,128)(2,1)S(1)} %get-tuple-element.157, bf16[4,512,2,64]{1,3,2,0:T(8,128)(2,1)S(1)} %get-tuple-element.156, s32[]{:T(128)} %get-tuple-element.146), kind=kOutput, calls=%fused_computation.69.clone.1 | convolution fusion | flops 274728960 | bytes 9048068 | tf_op jit(solution)/shard_map/while/body/eval_jaxpr/sub | solution.py:79
  51.3 4.4 %broadcast_divide_fusion.2 = f32[2,512,2048]{2,1,0:T(8,128)S(1)} fusion(f32[2,512,2048]{2,1,0:T(8,128)} %get-tuple-element.134, f32[2,512]{1,0:T(2,128)S(1)} %get-tuple-element.135), kind=kLoop, calls=%fused_computation.10.clone.1 | loop fusion | flops 2097152 | bytes 16781312 | tf_op jit(solution)/shard_map/while/body/eval_jaxpr/div | solution.py:79
  55.7 1.4 multiply_reduce_fusion.5
  57.3 0.1 copy.68
  57.4 0.7 constant_dynamic-update-slice_fusion.2
  58.0 4.9 %fusion.74 = (f32[2,512]{1,0:T(2,128)S(1)}, f32[2,512,2048]{2,1,0:T(8,128)}) fusion(bf16[2048,2,64]{0,2,1:T(8,128)(2,1)S(1)} %get-tuple-element.157, bf16[4,512,2,64]{1,3,2,0:T(8,128)(2,1)S(1)} %get-tuple-element.156, s32[]{:T(128)} %get-tuple-element.146), kind=kOutput, calls=%fused_computation.69.clone.1 | convolution fusion | flops 274728960 | bytes 9048068 | tf_op jit(solution)/shard_map/while/body/eval_jaxpr/sub | solution.py:79
  63.0 4.4 %broadcast_divide_fusion.2 = f32[2,512,2048]{2,1,0:T(8,128)S(1)} fusion(f32[2,512,2048]{2,1,0:T(8,128)} %get-tuple-element.134, f32[2,512]{1,0:T(2,128)S(1)} %get-tuple-element.135), kind=kLoop, calls=%fused_computation.10.clone.1 | loop fusion | flops 2097152 | bytes 16781312 | tf_op jit(solution)/shard_map/while/body/eval_jaxpr/div | solution.py:79
  67.4 1.4 multiply_reduce_fusion.5
  68.9 0.1 copy.68
  69.0 0.7 constant_dynamic-update-slice_fusion.2
  69.7 4.9 %fusion.74 = (f32[2,512]{1,0:T(2,128)S(1)}, f32[2,512,2048]{2,1,0:T(8,128)}) fusion(bf16[2048,2,64]{0,2,1:T(8,128)(2,1)S(1)} %get-tuple-element.157, bf16[4,512,2,64]{1,3,2,0:T(8,128)(2,1)S(1)} %get-tuple-element.156, s32[]{:T(128)} %get-tuple-element.146), kind=kOutput, calls=%fused_computation.69.clone.1 | convolution fusion | flops 274728960 | bytes 9048068 | tf_op jit(solution)/shard_map/while/body/eval_jaxpr/sub | solution.py:79
  74.6 4.4 %broadcast_divide_fusion.2 = f32[2,512,2048]{2,1,0:T(8,128)S(1)} fusion(f32[2,512,2048]{2,1,0:T(8,128)} %get-tuple-element.134, f32[2,512]{1,0:T(2,128)S(1)} %get-tuple-element.135), kind=kLoop, calls=%fused_computation.10.clone.1 | loop fusion | flops 2097152 | bytes 16781312 | tf_op jit(solution)/shard_map/while/body/eval_jaxpr/div | solution.py:79
  79.0 1.4 multiply_reduce_fusion.5
  80.6 0.1 copy.68
  80.7 0.7 constant_dynamic-update-slice_fusion.2
  81.4 4.9 %fusion.74 = (f32[2,512]{1,0:T(2,128)S(1)}, f32[2,512,2048]{2,1,0:T(8,128)}) fusion(bf16[2048,2,64]{0,2,1:T(8,128)(2,1)S(1)} %get-tuple-element.157, bf16[4,512,2,64]{1,3,2,0:T(8,128)(2,1)S(1)} %get-tuple-element.156, s32[]{:T(128)} %get-tuple-element.146), kind=kOutput, calls=%fused_computation.69.clone.1 | convolution fusion | flops 274728960 | bytes 9048068 | tf_op jit(solution)/shard_map/while/body/eval_jaxpr/sub | solution.py:79
  86.3 4.4 %broadcast_divide_fusion.2 = f32[2,512,2048]{2,1,0:T(8,128)S(1)} fusion(f32[2,512,2048]{2,1,0:T(8,128)} %get-tuple-element.134, f32[2,512]{1,0:T(2,128)S(1)} %get-tuple-element.135), kind=kLoop, calls=%fused_computation.10.clone.1 | loop fusion | flops 2097152 | bytes 16781312 | tf_op jit(solution)/shard_map/while/body/eval_jaxpr/div | solution.py:79
  90.7 1.4 multiply_reduce_fusion.5
  92.3 0.1 copy.68
  92.4 0.7 constant_dynamic-update-slice_fusion.2
  93.1 3.5 %all-to-all-start.1 = ((bf16[4,4,1,128,128]{4,3,1,2,0:T(8,128)(2,1)}), bf16[4,4,1,128,128]{4,3,1,2,0:T(8,128)(2,1)S(1)}, u32[]{:S(2)}, u32[]{:S(2)}) async-start(bf16[4,4,1,128,128]{4,3,1,2,0:T(8,128)(2,1)} %bitcast.8), calls=%async_computation.1 | async-start | bytes 1048576 | tf_op jit(solution)/shard_map/all_to_all | solution.py:47
  96.6 0.1 eq.25
  96.7 0.1 copy.54
  96.8 0.1 mul.103
  97.0 0.2 fusion.47
  97.2 6.8 %all-to-all-done.1 = bf16[4,4,1,128,128]{4,3,1,2,0:T(8,128)(2,1)S(1)} async-done(((bf16[4,4,1,128,128]{4,3,1,2,0:T(8,128)(2,1)}), bf16[4,4,1,128,128]{4,3,1,2,0:T(8,128)(2,1)S(1)}, u32[]{:S(2)}, u32[]{:S(2)}) %all-to-all-start.1) | async-done | bytes 524320 | tf_op jit(solution)/shard_map/all_to_all | solution.py:47
  104.0 0.8 copy.51
  104.8 3.5 %all-to-all-start.2 = ((bf16[4,4,1,128,128]{4,3,0,2,1:T(8,128)(2,1)}), bf16[4,4,1,128,128]{4,3,0,2,1:T(8,128)(2,1)S(1)}, u32[]{:S(2)}, u32[]{:S(2)}) async-start(bf16[4,4,1,128,128]{4,3,0,2,1:T(8,128)(2,1)} %copy.51), calls=%async_computation.2 | async-start | bytes 1048576 | tf_op jit(solution)/shard_map/all_to_all | solution.py:47
  108.3 1.4 scatter_custom_fusion
  109.8 5.5 %all-to-all-done.2 = bf16[4,4,1,128,128]{4,3,0,2,1:T(8,128)(2,1)S(1)} async-done(((bf16[4,4,1,128,128]{4,3,0,2,1:T(8,128)(2,1)}), bf16[4,4,1,128,128]{4,3,0,2,1:T(8,128)(2,1)S(1)}, u32[]{:S(2)}, u32[]{:S(2)}) %all-to-all-start.2) | async-done | bytes 524320 | tf_op jit(solution)/shard_map/all_to_all | solution.py:47
  115.3 0.3 copy.53
  115.6 4.7 %multiply_reduce_fusion.3 = (f32[128]{0:T(128)S(1)}, f32[128,2048]{1,0:T(8,128)S(1)}) fusion(bf16[128,2048]{0,1:T(8,128)(2,1)S(1)} %bitcast.118, bf16[2048,2048]{1,0:T(8,128)(2,1)} %param.21, bf16[1,128,2048]{2,1,0:T(8,128)(2,1)S(1)} %copy-done.1), kind=kOutput, calls=%fused_computation.44 | convolution fusion | flops 1075314560 | bytes 10486272 | tf_op jit(solution)/shard_map/dot_general | solution.py:116
  120.3 0.2 multiply_convert_fusion.2
  120.6 3.3 %gather_fusion = bf16[512,2048]{1,0:T(8,128)(2,1)} fusion(bf16[129,2048]{1,0:T(8,128)(2,1)S(1)} %concatenate.7, s32[1024]{0:T(1024)S(1)} %pad_clamp_fusion.1), kind=kCustom, calls=%fused_computation | custom fusion | bytes 4196352 | tf_op jit(solution)/shard_map/gather | solution.py:136
  123.9 2.7 %reshape_transpose_transpose_reshape_reshape_reshape_reshape.3 = bf16[128,1,1,4,2048]{4,3,0,2,1:T(4,128)(2,1)S(1)} reshape(bf16[512,2048]{1,0:T(8,128)(2,1)} %gather_fusion) | data formatting | bytes 4194304 | tf_op jit(solution)/shard_map/reshape;transpose;transpose;reshape;reshape;reshape;reshape | solution.py:61
  126.6 39.5 %all_to_all.35 = bf16[128,1,1,4,2048]{4,3,2,1,0:T(4,128)(2,1)} all-to-all(bf16[128,1,1,4,2048]{4,3,2,1,0:T(4,128)(2,1)S(1)} %bitcast.115), channel_id=1, replica_groups=mesh['sp_0'=4,'sp_1'=4,'dp'=8] {'sp_0','sp_1','dp'}, dimensions={0} | all-to-all | bytes 4194304 | tf_op jit(solution)/shard_map/all_to_all | solution.py:62
  166.2 2.5 %reshape_reshape.6 = bf16[512,2048]{1,0:T(8,128)(2,1)S(1)} reshape(bf16[16,8,1,4,2048]{4,3,1,0,2:T(4,128)(2,1)} %bitcast.116) | data formatting | bytes 4194304 | tf_op jit(solution)/shard_map/reshape;reshape | solution.py:139
  168.7 5.8 %fusion.33 = f32[512,1024]{1,0:T(8,128)} fusion(bf16[512,2048]{1,0:T(8,128)(2,1)S(1)} %reshape_reshape.6, bf16[1,2048,1024]{2,1,0:T(8,128)(2,1)} %param.25), kind=kOutput, calls=%fused_computation.32 | convolution fusion | flops 2147483648 | bytes 8388608 | tf_op jit(solution)/shard_map/dot_general | solution.py:140
  174.5 10.0 %fusion.35 = bf16[512,2048]{1,0:T(8,128)(2,1)} fusion(bf16[1,1024,2048]{2,1,0:T(8,128)(2,1)} %param.27, f32[512,1024]{1,0:T(8,128)} %fusion.33, bf16[512,2048]{1,0:T(8,128)(2,1)S(1)} %reshape_reshape.6, bf16[1,2048,1024]{2,1,0:T(8,128)(2,1)} %param.26), kind=kOutput, calls=%fused_computation.34 | convolution fusion | flops 4299161600 | bytes 14680064 | tf_op jit(solution)/shard_map/dot_general | solution.py:143
  184.5 4.1 %reshape_transpose_transpose_reshape_reshape_reshape.3 = bf16[128,1,1,4,2048]{4,3,0,2,1:T(4,128)(2,1)} reshape(bf16[512,2048]{1,0:T(8,128)(2,1)} %fusion.35) | data formatting | bytes 4194304 | tf_op jit(solution)/shard_map/reshape;transpose;transpose;reshape;reshape;reshape | solution.py:61
  188.6 4.5 %all-to-all-start.4 = ((bf16[128,1,1,4,2048]{4,3,2,1,0:T(4,128)(2,1)}), bf16[128,1,1,4,2048]{4,3,2,1,0:T(4,128)(2,1)S(1)}, u32[]{:S(2)}, u32[]{:S(2)}) async-start(bf16[128,1,1,4,2048]{4,3,2,1,0:T(4,128)(2,1)} %bitcast.114), calls=%async_computation.4 | async-start | bytes 4194304 | tf_op jit(solution)/shard_map/all_to_all | solution.py:62
  193.3 30.5 %all-to-all-done.4 = bf16[128,1,1,4,2048]{4,3,2,1,0:T(4,128)(2,1)S(1)} async-done(((bf16[128,1,1,4,2048]{4,3,2,1,0:T(4,128)(2,1)}), bf16[128,1,1,4,2048]{4,3,2,1,0:T(4,128)(2,1)S(1)}, u32[]{:S(2)}, u32[]{:S(2)}) %all-to-all-start.4) | async-done | bytes 2097184 | tf_op jit(solution)/shard_map/all_to_all | solution.py:62
  223.8 1.3 copy-done
  225.1 2.5 %reshape_reshape.7 = bf16[512,2048]{1,0:T(8,128)(2,1)S(1)} reshape(bf16[16,8,1,4,2048]{4,3,1,0,2:T(4,128)(2,1)} %bitcast.113) | data formatting | bytes 4194304 | tf_op jit(solution)/shard_map/reshape;reshape | solution.py:147
  227.7 2.3 gather_fusion.1
  230.0 2.4 %reshape.109 = f32[128,2,2048]{2,1,0:T(2,128)S(1)} reshape(bf16[256,2048]{1,0:T(8,128)(2,1)} %gather_fusion.1) | data formatting | bytes 3145728 | tf_op jit(solution)/shard_map/convert_element_type | solution.py:148
  232.4 3.2 %multiply_reduce_fusion.2 = f32[128,2048]{1,0:T(8,128)S(1)} fusion(f32[128,2,2048]{2,1,0:T(2,128)S(1)} %reshape.109, f32[128,2]{1,0:T(8,128)S(1)} %copy.61), kind=kLoop, calls=%fused_computation.38 | loop fusion | flops 786432 | bytes 3146752 | tf_op jit(solution)/shard_map/reduce_sum | solution.py:151
  235.6 0.9 fusion.44
  (37 shorter events, 0.8 us)
Async XLA Ops:
  4.1 8.8 %copy-start.3 = (s32[1,128,2]{1,2,0:T(2,128)S(1)}, s32[1,128,2]{1,2,0:T(2,128)}, u32[]{:S(2)}) copy-start(s32[1,128,2]{1,2,0:T(2,128)} %param.23) | copy-start | bytes 3076
  4.1 10.2 %copy-start.5 = (f32[16]{0:T(128)S(1)}, f32[16]{0:T(128)}, u32[]{:S(2)}) copy-start(f32[16]{0:T(128)} %param.19) | copy-start | bytes 196
  4.1 39.7 %all-to-all-start = ((bf16[3,128,2048]{1,0,2:T(4,128)(2,1)}), bf16[3,128,2048]{1,0,2:T(4,128)(2,1)S(1)}, u32[]{:S(2)}, u32[]{:S(2)}) async-start(bf16[3,128,2048]{1,0,2:T(4,128)(2,1)} %copy.46), calls=%async_computation | async-start | bytes 4194304 | tf_op jit(solution)/shard_map/all_to_all | solution.py:21
  93.1 10.9 %all-to-all-start.1 = ((bf16[4,4,1,128,128]{4,3,1,2,0:T(8,128)(2,1)}), bf16[4,4,1,128,128]{4,3,1,2,0:T(8,128)(2,1)S(1)}, u32[]{:S(2)}, u32[]{:S(2)}) async-start(bf16[4,4,1,128,128]{4,3,1,2,0:T(8,128)(2,1)} %bitcast.8), calls=%async_computation.1 | async-start | bytes 1048576 | tf_op jit(solution)/shard_map/all_to_all | solution.py:47
  97.2 18.4 %copy-start.1 = (bf16[1,128,2048]{2,1,0:T(8,128)(2,1)S(1)}, bf16[1,128,2048]{2,1,0:T(8,128)(2,1)}, u32[]{:S(2)}) copy-start(bf16[1,128,2048]{2,1,0:T(8,128)(2,1)} %param.15) | copy-start | bytes 1572868
  104.8 10.4 %all-to-all-start.2 = ((bf16[4,4,1,128,128]{4,3,0,2,1:T(8,128)(2,1)}), bf16[4,4,1,128,128]{4,3,0,2,1:T(8,128)(2,1)S(1)}, u32[]{:S(2)}, u32[]{:S(2)}) async-start(bf16[4,4,1,128,128]{4,3,0,2,1:T(8,128)(2,1)} %copy.51), calls=%async_computation.2 | async-start | bytes 1048576 | tf_op jit(solution)/shard_map/all_to_all | solution.py:47
  115.6 4.8 %copy-start.2 = (f32[2048]{0:T(1024)S(1)}, f32[2048]{0:T(1024)}, u32[]{:S(2)}) copy-start(f32[2048]{0:T(1024)} %param.22) | copy-start | bytes 24580
  188.6 4.6 %copy-start.4 = (f32[1,128,2]{1,2,0:T(2,128)S(1)}, f32[1,128,2]{1,2,0:T(2,128)}, u32[]{:S(2)}) copy-start(f32[1,128,2]{1,2,0:T(2,128)} %param.24) | copy-start | bytes 3076
  188.6 35.2 %all-to-all-start.4 = ((bf16[128,1,1,4,2048]{4,3,2,1,0:T(4,128)(2,1)}), bf16[128,1,1,4,2048]{4,3,2,1,0:T(4,128)(2,1)S(1)}, u32[]{:S(2)}, u32[]{:S(2)}) async-start(bf16[128,1,1,4,2048]{4,3,2,1,0:T(4,128)(2,1)} %bitcast.114), calls=%async_computation.4 | async-start | bytes 4194304 | tf_op jit(solution)/shard_map/all_to_all | solution.py:62
  223.8 1.4 copy-start
where the time goes:
time: 237 us
  waiting for transfers between devices  71.7 us (30%)
  matrix products  45.9 us (19%)
  blocking collectives  39.5 us (17%)
  local copies, waits for them, and re-layouts  34.4 us (15%)
  other arithmetic  24.3 us (10%)
  starting transfers between devices  20.2 us (9%)
    all_to_all x1, blocking collectives, exchange_both(): lax.all_to_all(blocks, axis, split_axis=0, concat_axis=0, tiled=True)  39.5 us
    all_to_all x1, waiting for transfers between devices, exchange_both(): lax.all_to_all(blocks, axis, split_axis=0, concat_axis=0, tiled=True)  30.5 us
    all_to_all x1, waiting for transfers between devices, side_by_side(): lax.all_to_all(both, axis, split_axis=split_dim, concat_axis=concat_dim,...  29 us
    sub x4, matrix products, one_block(): probabilities = jax.nn.softmax(scores, axis=-1)  19.6 us
    div x4, other arithmetic, one_block(): probabilities = jax.nn.softmax(scores, axis=-1)  17.6 us
    all_to_all x2, waiting for transfers between devices, exchange_in_order(): lax.all_to_all(blocks, axes[k], split_axis=k, concat_axis=k, tiled=True)  12.3 us
    dot_general x1, matrix products, on_device(): jnp.dot(hidden, expert_down[0], preferred_element_type=jnp.float32)  9.95 us
    all_to_all x1, starting transfers between devices, side_by_side(): lax.all_to_all(both, axis, split_axis=split_dim, concat_axis=concat_dim,...  8.72 us
  transfers between devices with their start and end apart: 4, of which 4 were waited for; matrix products, arithmetic and copies ran while one was open for 2% of the time, Pallas kernels for 0%

commit v1 on v0

v1 whole, which is shorter than its diff:
```python
import jax
import jax.numpy as jnp
from jax import lax
from jax.experimental import pallas as pl
from jax.experimental.pallas import tpu as pltpu
from jax.sharding import PartitionSpec as P

D = 2048
HEADS = 16
HD = 64
VD = 128
TOK = 128
SEQ = 2048
QB = 256
STEPS = SEQ // QB
KC = 256
RB = 16
MESH = pl.DeviceIdType.MESH
SP_DP = ("sp", "dp")
eps = 1e-06
LOG2E = 1.4426950408889634
NEAR = {0: 0, 1: 1, 2: 2, 3: 1}
PEERS = sorted(
    [(a, b) for a in range(4) for b in range(4) if (a, b) != (0, 0)],
    key=lambda o: -(NEAR[o[0]] + NEAR[o[1]]),
)


def peer_of(me, off):
    return ((me // 4 + off[0]) % 4) * 4 + (me % 4 + off[1]) % 4


def source_of(me, off):
    return ((me // 4 + 4 - off[0]) % 4) * 4 + (me % 4 + 4 - off[1]) % 4


def cols(block):
    return pl.ds(pl.multiple_of(block * VD, VD), VD)


def attention_kernel(
    q_ref, k_ref, v_ref, lam_ref, gain_ref, att_ref,
    qa, ka, va, s1a, s2a, s1b, s2b, pbuf, obuf,
    qs, ks, vs, qr, kr, vr, os_, or_, lsem,
):
    me = lax.axis_index("sp")
    barrier = pltpu.get_barrier_semaphore()
    for off in PEERS:
        pl.semaphore_signal(barrier, inc=1, device_id={"sp": peer_of(me, off)}, device_id_type=MESH)
    pl.semaphore_wait(barrier, len(PEERS))
    mine = cols(me)
    sends = []
    for n, (src, dst, ss, rs) in enumerate(((k_ref, ka, ks, kr), (v_ref, va, vs, vr), (q_ref, qa, qs, qr))):
        for i, off in enumerate(PEERS):
            to = peer_of(me, off)
            copy = pltpu.make_async_remote_copy(
                src.at[:, cols(to)], dst.at[mine, :], ss.at[i], rs.at[i],
                device_id={"sp": to}, device_id_type=MESH,
            )
            copy.start()
            sends.append(copy)
        own = pltpu.make_async_copy(src.at[:, mine], dst.at[mine, :], lsem.at[n])
        own.start()
        own.wait()
    count = len(PEERS)
    for copy in sends[: 2 * count]:
        copy.wait_recv()
    for copy in sends[2 * count :]:
        copy.wait_recv()
    lam = lam_ref[me]
    gain = gain_ref[pl.ds(me, 1), :] * 0.8
    first = lax.broadcasted_iota(jnp.int32, (QB, VD), 1) < HD
    scale = HD ** (-0.5) * LOG2E

    def scores(step, s1, s2):
        q = qa[pl.ds(pl.multiple_of(step * QB, QB), QB), :]
        zero = jnp.zeros_like(q)
        q1 = jnp.where(first, q, zero)
        q2 = jnp.where(first, zero, q)
        for c in range(SEQ // KC):
            k = ka[c * KC : (c + 1) * KC, :]
            at = pl.ds(c * KC, KC)
            dims = (((1,), (1,)), ((), ()))
            s1[:, at] = lax.dot_general(q1, k, dims, preferred_element_type=jnp.float32)
            s2[:, at] = lax.dot_general(q2, k, dims, preferred_element_type=jnp.float32)

    def mixed(step, s1, s2):
        inv = []
        for r in range(QB // RB):
            at = pl.ds(r * RB, RB)
            a = s1[at, :]
            e1 = jnp.exp2((a - jnp.max(a, axis=1, keepdims=True)) * scale)
            l1 = jnp.sum(e1, axis=1, keepdims=True)
            b = s2[at, :]
            e2 = jnp.exp2((b - jnp.max(b, axis=1, keepdims=True)) * scale)
            l2 = jnp.sum(e2, axis=1, keepdims=True)
            pbuf[at, :] = (e1 - e2 * (lam * l1 / l2)).astype(jnp.bfloat16)
            inv.append(1.0 / l1)
        out = jnp.dot(pbuf[...], va[...], preferred_element_type=jnp.float32)
        out = out * jnp.concatenate(inv, axis=0)
        out = out * lax.rsqrt(jnp.mean(out * out, axis=1, keepdims=True) + eps) * gain
        obuf[pl.ds(pl.multiple_of(step * QB, QB), QB), :] = out.astype(jnp.bfloat16)

    def pair(i, carry):
        step = 2 * i
        scores(step + 1, s1b, s2b)
        mixed(step, s1a, s2a)
        scores((step + 2) % STEPS, s1a, s2a)
        mixed(step + 1, s1b, s2b)
        return carry

    scores(0, s1a, s2a)
    lax.fori_loop(0, STEPS // 2, pair, 0)
    outs = []
    for i, off in enumerate(PEERS):
        to = peer_of(me, off)
        copy = pltpu.make_async_remote_copy(
            obuf.at[cols(to), :], att_ref.at[:, mine], os_.at[i], or_.at[i],
            device_id={"sp": to}, device_id_type=MESH,
        )
        copy.start()
        outs.append(copy)
    own = pltpu.make_async_copy(obuf.at[mine, :], att_ref.at[:, mine], lsem.at[3])
    own.start()
    own.wait()
    for copy in outs:
        copy.wait_recv()
    for copy in sends + outs:
        copy.wait_send()


def attention(q, k, v, lambdas, gain):
    n = len(PEERS)
    vmem = pl.BlockSpec(memory_space=pltpu.VMEM)
    smem = pl.BlockSpec(memory_space=pltpu.SMEM)
    score = pltpu.VMEM((QB, SEQ), jnp.float32)
    rows = pltpu.VMEM((SEQ, VD), jnp.bfloat16)
    return pl.pallas_call(
        attention_kernel,
        out_shape=jax.ShapeDtypeStruct((TOK, D), jnp.bfloat16),
        in_specs=[vmem, vmem, vmem, smem, vmem],
        out_specs=vmem,
        scratch_shapes=[rows, rows, rows, score, score, score, score,
                        pltpu.VMEM((QB, SEQ), jnp.bfloat16), rows]
        + [pltpu.SemaphoreType.DMA((n,))] * 8 + [pltpu.SemaphoreType.DMA((4,))],
        compiler_params=pltpu.CompilerParams(
            collective_id=0, has_side_effects=True, vmem_limit_bytes=56 * 2**20
        ),
        name="attention",
    )(q, k, v, lambdas, gain)


def in_blocks(value, dim, size):
    lengths = value.shape
    blocks = value.reshape(*lengths[:dim], size, lengths[dim] // size, *lengths[dim + 1 :])
    return jnp.moveaxis(blocks, dim, 0)


def laid_out(blocks, dim):
    blocks = jnp.moveaxis(blocks, 0, dim)
    lengths = blocks.shape
    return blocks.reshape(*lengths[:dim], lengths[dim] * lengths[dim + 1], *lengths[dim + 2 :])


def exchange_both(value, axis, axes, splits, concats):
    sizes = [lax.axis_size(a) for a in axes]
    blocks = in_blocks(value, splits[0], sizes[0])
    blocks = jnp.moveaxis(in_blocks(blocks, splits[1] + 1, sizes[1]), 0, 1)
    inside = blocks.shape[2:]
    blocks = blocks.reshape(-1, *inside)
    blocks = lax.all_to_all(blocks, axis, split_axis=0, concat_axis=0, tiled=True)
    blocks = laid_out(blocks.reshape(*sizes, *inside), concats[0] + 1)
    return laid_out(blocks, concats[1])


def on_device(
    residual, query_maps, key_maps, value_rows, lambdas, head_gain, out_weight, ffn_gain,
    routes, route_weights, expert_gate, expert_up, expert_down,
):
    count_sp = lax.axis_size("sp")
    count_dp = lax.axis_size("dp")
    returned_heads = attention(
        query_maps[0], key_maps[0], value_rows[0], lambdas, head_gain.reshape(HEADS, VD)
    )
    projected = jnp.dot(returned_heads, out_weight, preferred_element_type=jnp.float32)
    residual_mid = (residual[0].astype(jnp.float32) + projected).astype(jnp.bfloat16)
    middle = residual_mid.astype(jnp.float32)
    expert_input = (
        middle * lax.rsqrt(jnp.mean(middle * middle, axis=-1, keepdims=True) + eps) * ffn_gain
    ).astype(jnp.bfloat16)
    tok_rows = residual.shape[1]
    experts_all = count_sp * count_dp
    capacity = max(2, 4 * tok_rows // experts_all)
    flat_routes = routes[0].reshape(-1)
    flat_weights = route_weights[0].reshape(-1)
    onehot = (flat_routes[:, None] == jnp.arange(experts_all, dtype=jnp.int32)[None, :]).astype(
        jnp.int32
    )
    before = jnp.cumsum(onehot, axis=0) - onehot
    rank_of = jnp.sum(before * onehot, axis=1)
    slot = flat_routes * capacity + rank_of
    token_of = jnp.arange(flat_routes.shape[0], dtype=jnp.int32) // routes.shape[2]
    slot_token = jnp.full((experts_all * capacity,), tok_rows, jnp.int32).at[slot].set(token_of)
    padded_input = jnp.concatenate([expert_input, jnp.zeros((1, D), jnp.bfloat16)], axis=0)
    buffer = padded_input[slot_token].reshape(experts_all, capacity, D)
    shaped = buffer.reshape(count_sp, count_dp, capacity, D)
    received = exchange_both(shaped, SP_DP, ("sp", "dp"), (0, 1), (0, 1))
    row_block = received.reshape(-1, D)
    gate_part = jnp.dot(row_block, expert_gate[0], preferred_element_type=jnp.float32)
    up_part = jnp.dot(row_block, expert_up[0], preferred_element_type=jnp.float32)
    hidden = (jax.nn.silu(gate_part) * up_part).astype(jnp.bfloat16)
    expert_out = jnp.dot(hidden, expert_down[0], preferred_element_type=jnp.float32).astype(
        jnp.bfloat16
    )
    returned = exchange_both(expert_out.reshape(received.shape), SP_DP, ("sp", "dp"), (0, 1), (0, 1))
    picked = returned.reshape(experts_all * capacity, D)[slot]
    weighted = (picked.astype(jnp.float32) * flat_weights[:, None]).reshape(
        tok_rows, routes.shape[2], D
    )
    layer_out = (middle + jnp.sum(weighted, axis=1)).astype(jnp.bfloat16)
    return layer_out[None]


def solution(mesh):
    tokens = P("dp", "sp", None)
    experts = P(SP_DP, None, None)
    placed = (tokens,) * 4 + (P(),) * 4 + (tokens,) * 2 + (experts,) * 3
    return jax.shard_map(
        on_device, mesh=mesh, in_specs=placed, out_specs=tokens, check_vma=False
    )
```

time: 237 us -> 175 us (0.74)
  Pallas kernels: 0 us -> 49.9 us
  waiting for transfers between devices: 71.7 us -> 30.5 us
  matrix products: 45.9 us -> 20.7 us
  other arithmetic: 24.3 us -> 5.41 us
  starting transfers between devices: 20.2 us -> 4.55 us
  local copies, waits for them, and re-layouts: 34.4 us -> 24.4 us
    pallas_call x0 -> x1, Pallas kernels: none -> 49.9 us  [attention(): pl.pallas_call(attention_kernel, out_shape=jax.ShapeDtypeStruct((TOK, D),...]
    all_to_all x3 -> x0, waiting for transfers between devices: 41.3 us -> none  [the longest x1 29 us: side_by_side(): lax.all_to_all(both, axis, split_axis=split_dim, concat_axis=concat_dim,...]
    sub x4 -> x0, matrix products: 19.6 us -> none  [one_block(): probabilities = jax.nn.softmax(scores, axis=-1)]
    div x4 -> x0, other arithmetic: 17.6 us -> none  [one_block(): probabilities = jax.nn.softmax(scores, axis=-1)]
    all_to_all x3 -> x0, starting transfers between devices: 15.7 us -> none  [the longest x1 8.72 us: side_by_side(): lax.all_to_all(both, axis, split_axis=split_dim, concat_axis=concat_dim,...]
    dot_general x5 -> x1, matrix products: 10.5 us -> 4.96 us  [on_device(): jnp.dot(returned_heads, out_weight, preferred_element_type=jnp.float32)]
    dynamic_update_slice x8 -> x0, local copies, waits for them, and re-layouts: 3.15 us -> none  [attend_head(): lax.map(one_block, query_blocks).reshape(length, value_head.shape[-1])]
    concatenate x1 -> x0, local copies, waits for them, and re-layouts: 2.54 us -> none  [side_by_side(): both = jnp.concatenate(arrays, axis=along)]
  transfers between devices with their start and end apart: 4 -> 1, of which waited for: 4 -> 1; matrix products, arithmetic and copies ran while one was open for 2% -> 0% of each run, Pallas kernels for 0% -> 0%
where the time goes in v1:
time: 175 us; the launch traced here: 174 us
  Pallas kernels  49.9 us (29%)
  blocking collectives  38.6 us (22%)
  waiting for transfers between devices  30.5 us (17%)
  local copies, waits for them, and re-layouts  24.4 us (14%)
  matrix products  20.7 us (12%)
  other arithmetic  5.41 us (3%)
  starting transfers between devices  4.55 us (3%)
    pallas_call x1, Pallas kernels, attention(): pl.pallas_call(attention_kernel, out_shape=jax.ShapeDtypeStruct((TOK, D),...  49.9 us
    all_to_all x1, blocking collectives, exchange_both(): lax.all_to_all(blocks, axis, split_axis=0, concat_axis=0, tiled=True)  38.6 us
    all_to_all x1, waiting for transfers between devices, exchange_both(): lax.all_to_all(blocks, axis, split_axis=0, concat_axis=0, tiled=True)  30.5 us
    dot_general x1, matrix products, on_device(): jnp.dot(hidden, expert_down[0], preferred_element_type=jnp.float32)  9.95 us
    another operation x2, local copies, waits for them, and re-layouts, exchange_both(): blocks = blocks.reshape(-1, *inside)  6.85 us
    dot_general x1, matrix products, on_device(): jnp.dot(row_block, expert_gate[0], preferred_element_type=jnp.float32)  5.81 us
    dot_general x1, matrix products, on_device(): jnp.dot(returned_heads, out_weight, preferred_element_type=jnp.float32)  4.96 us
    all_to_all x1, starting transfers between devices, exchange_both(): lax.all_to_all(blocks, axis, split_axis=0, concat_axis=0, tiled=True)  4.55 us
  transfers between devices with their start and end apart: 1, of which 1 were waited for; matrix products, arithmetic and copies ran while one was open for 0% of the time, Pallas kernels for 0%

profile of v1, /device:TPU:1, one launch (start us, length us, event | category | flops | bytes accessed | tf_op | source)
XLA Modules:
  0.0 174.2 jit_solution(984076891915046095)
XLA Ops:
  0.0 0.0 copy-start.1
  0.0 0.8 copy.22
  0.8 0.1 eq.29
  1.0 0.1 eq.25
  1.1 0.7 broadcast_multiply_fusion
  1.8 0.1 copy.24
  1.9 0.2 fusion.16
  2.2 0.1 copy.21
  2.3 0.1 mul.63
  2.5 0.2 fusion.18
  2.7 1.4 scatter_custom_fusion
  4.1 49.9 %attention.1 = bf16[128,2048]{1,0:T(8,128)(2,1)} custom-call(bf16[128,2048]{1,0:T(8,128)(2,1)} %bitcast.69, bf16[128,2048]{1,0:T(8,128)(2,1)} %bitcast.70, bf16[128,2048]{1,0:T(8,128)(2,1)} %bitcast.71, f32[16]{0:T(128)} %lam_ref.1, f32[16,128]{1,0:T(8,128)} %bitcast.74), custom_call_target="tpu_custom_call" | custom-call | tf_op jit(solution)/shard_map/attention/pallas_call | solution.py:138
  54.0 0.0 copy-done.1
  54.0 0.0 copy-start.2
  54.0 5.0 %multiply_reduce_fusion.1 = (f32[128]{0:T(128)S(1)}, f32[128,2048]{1,0:T(8,128)S(1)}) fusion(bf16[128,2048]{1,0:T(8,128)(2,1)} %attention.1, bf16[2048,2048]{1,0:T(8,128)(2,1)} %param.19, bf16[1,128,2048]{2,1,0:T(8,128)(2,1)S(1)} %copy-done.1), kind=kOutput, calls=%fused_computation.17 | convolution fusion | flops 1075314560 | bytes 10486272 | tf_op jit(solution)/shard_map/dot_general | solution.py:185
  59.0 0.0 copy-done.2
  59.0 0.2 multiply_convert_fusion.1
  59.2 3.3 %gather_fusion = bf16[512,2048]{1,0:T(8,128)(2,1)} fusion(bf16[129,2048]{1,0:T(8,128)(2,1)S(1)} %concatenate.3, s32[1024]{0:T(1024)S(1)} %pad_clamp_fusion.1), kind=kCustom, calls=%fused_computation | custom fusion | bytes 4196352 | tf_op jit(solution)/shard_map/gather | solution.py:205
  62.5 2.7 %reshape_transpose_transpose_reshape_reshape_reshape_reshape.3 = bf16[128,1,1,4,2048]{4,3,0,2,1:T(4,128)(2,1)S(1)} reshape(bf16[512,2048]{1,0:T(8,128)(2,1)} %gather_fusion) | data formatting | bytes 4194304 | tf_op jit(solution)/shard_map/reshape;transpose;transpose;reshape;reshape;reshape;reshape | solution.py:170
  65.3 38.6 %all_to_all.10 = bf16[128,1,1,4,2048]{4,3,2,1,0:T(4,128)(2,1)} all-to-all(bf16[128,1,1,4,2048]{4,3,2,1,0:T(4,128)(2,1)S(1)} %bitcast.66), channel_id=1, replica_groups=mesh['sp'=16,'dp'=8] {'sp','dp'}, dimensions={0} | all-to-all | bytes 4194304 | tf_op jit(solution)/shard_map/all_to_all | solution.py:171
  103.9 2.5 %reshape_reshape.6 = bf16[512,2048]{1,0:T(8,128)(2,1)S(1)} reshape(bf16[16,8,1,4,2048]{4,3,1,0,2:T(4,128)(2,1)} %bitcast.67) | data formatting | bytes 4194304 | tf_op jit(solution)/shard_map/reshape;reshape | solution.py:208
  106.5 5.8 %fusion.4 = f32[512,1024]{1,0:T(8,128)} fusion(bf16[512,2048]{1,0:T(8,128)(2,1)S(1)} %reshape_reshape.6, bf16[1,2048,1024]{2,1,0:T(8,128)(2,1)} %param.23), kind=kOutput, calls=%fused_computation.7 | convolution fusion | flops 2147483648 | bytes 8388608 | tf_op jit(solution)/shard_map/dot_general | solution.py:209
  112.3 10.0 %fusion.6 = bf16[512,2048]{1,0:T(8,128)(2,1)} fusion(bf16[1,1024,2048]{2,1,0:T(8,128)(2,1)} %param.25, f32[512,1024]{1,0:T(8,128)} %fusion.4, bf16[512,2048]{1,0:T(8,128)(2,1)S(1)} %reshape_reshape.6, bf16[1,2048,1024]{2,1,0:T(8,128)(2,1)} %param.24), kind=kOutput, calls=%fused_computation.9 | convolution fusion | flops 4299161600 | bytes 14680064 | tf_op jit(solution)/shard_map/dot_general | solution.py:212
  122.2 4.1 %reshape_transpose_transpose_reshape_reshape_reshape.3 = bf16[128,1,1,4,2048]{4,3,0,2,1:T(4,128)(2,1)} reshape(bf16[512,2048]{1,0:T(8,128)(2,1)} %fusion.6) | data formatting | bytes 4194304 | tf_op jit(solution)/shard_map/reshape;transpose;transpose;reshape;reshape;reshape | solution.py:170
  126.4 0.0 copy-start.3
  126.4 4.5 %all-to-all-start.1 = ((bf16[128,1,1,4,2048]{4,3,2,1,0:T(4,128)(2,1)}), bf16[128,1,1,4,2048]{4,3,2,1,0:T(4,128)(2,1)S(1)}, u32[]{:S(2)}, u32[]{:S(2)}) async-start(bf16[128,1,1,4,2048]{4,3,2,1,0:T(4,128)(2,1)} %bitcast.65), calls=%async_computation.1 | async-start | bytes 4194304 | tf_op jit(solution)/shard_map/all_to_all | solution.py:171
  130.9 0.0 copy-done.3
  130.9 0.1 copy.28
  131.0 30.5 %all-to-all-done.1 = bf16[128,1,1,4,2048]{4,3,2,1,0:T(4,128)(2,1)S(1)} async-done(((bf16[128,1,1,4,2048]{4,3,2,1,0:T(4,128)(2,1)}), bf16[128,1,1,4,2048]{4,3,2,1,0:T(4,128)(2,1)S(1)}, u32[]{:S(2)}, u32[]{:S(2)}) %all-to-all-start.1) | async-done | bytes 2097184 | tf_op jit(solution)/shard_map/all_to_all | solution.py:171
  161.5 0.0 copy-start
  161.5 1.3 copy-done
  162.9 2.5 %reshape_reshape.7 = bf16[512,2048]{1,0:T(8,128)(2,1)S(1)} reshape(bf16[16,8,1,4,2048]{4,3,1,0,2:T(4,128)(2,1)} %bitcast.64) | data formatting | bytes 4194304 | tf_op jit(solution)/shard_map/reshape;reshape | solution.py:216
  165.4 2.3 %gather_fusion.1 = bf16[256,2048]{1,0:T(8,128)(2,1)} fusion(bf16[512,2048]{1,0:T(8,128)(2,1)S(1)} %reshape_reshape.7, s32[1024]{0:T(1024)S(1)} %pad_clamp_fusion), kind=kCustom, calls=%fused_computation.1 | custom fusion | bytes 2098176 | tf_op jit(solution)/shard_map/gather | solution.py:216
  167.8 2.4 %reshape.88 = f32[128,2,2048]{2,1,0:T(2,128)S(1)} reshape(bf16[256,2048]{1,0:T(8,128)(2,1)} %gather_fusion.1) | data formatting | bytes 3145728 | tf_op jit(solution)/shard_map/convert_element_type | solution.py:217
  170.1 3.2 %multiply_reduce_fusion = f32[128,2048]{1,0:T(8,128)S(1)} fusion(f32[128,2,2048]{2,1,0:T(2,128)S(1)} %reshape.88, f32[128,2]{1,0:T(8,128)S(1)} %copy.28), kind=kLoop, calls=%fused_computation.13 | loop fusion | flops 786432 | bytes 3146752 | tf_op jit(solution)/shard_map/reduce_sum | solution.py:220
  173.3 0.9 fusion.15
  (13 shorter events, 0.2 us)
Async XLA Ops:
  0.0 54.0 %copy-start.1 = (bf16[1,128,2048]{2,1,0:T(8,128)(2,1)S(1)}, bf16[1,128,2048]{2,1,0:T(8,128)(2,1)}, u32[]{:S(2)}) copy-start(bf16[1,128,2048]{2,1,0:T(8,128)(2,1)} %param.13) | copy-start | bytes 1572868
  54.0 5.0 %copy-start.2 = (f32[2048]{0:T(1024)S(1)}, f32[2048]{0:T(1024)}, u32[]{:S(2)}) copy-start(f32[2048]{0:T(1024)} %param.20) | copy-start | bytes 24580
  126.4 4.6 %copy-start.3 = (f32[1,128,2]{1,2,0:T(2,128)S(1)}, f32[1,128,2]{1,2,0:T(2,128)}, u32[]{:S(2)}) copy-start(f32[1,128,2]{1,2,0:T(2,128)} %param.22) | copy-start | bytes 3076
  126.4 35.2 %all-to-all-start.1 = ((bf16[128,1,1,4,2048]{4,3,2,1,0:T(4,128)(2,1)}), bf16[128,1,1,4,2048]{4,3,2,1,0:T(4,128)(2,1)S(1)}, u32[]{:S(2)}, u32[]{:S(2)}) async-start(bf16[128,1,1,4,2048]{4,3,2,1,0:T(4,128)(2,1)} %bitcast.65), calls=%async_computation.1 | async-start | bytes 4194304 | tf_op jit(solution)/shard_map/all_to_all | solution.py:171
  161.5 1.4 copy-start

commit v2 on v1

v2 whole, which is shorter than its diff:
```python
import jax
import jax.numpy as jnp
from jax import lax
from jax.experimental import pallas as pl
from jax.experimental.pallas import tpu as pltpu
from jax.sharding import PartitionSpec as P

D = 2048
HEADS = 16
HD = 64
VD = 128
FF = 1024
TOK = 128
SEQ = 2048
EXPERTS = 128
CAP = 4
SLOTS = EXPERTS * CAP
QB = 256
STEPS = SEQ // QB
KC = 256
RB = 16
NC = 512
GROUP = 32
MESH = pl.DeviceIdType.MESH
eps = 1e-06
LOG2E = 1.4426950408889634
F32 = jnp.float32
BF16 = jnp.bfloat16
NEAR = {0: 0, 1: 1, 2: 2, 3: 1}
PEERS = sorted(
    [(a, b) for a in range(4) for b in range(4) if (a, b) != (0, 0)],
    key=lambda o: -(NEAR[o[0]] + NEAR[o[1]]),
)
INNER = [(a, b, c) for a in (2, 3, 0, 1) for b in (2, 3, 0, 1) for c in (0, 1)]
OWN_GROUP, OWN_AT = 2, INNER.index((0, 0, 0))


def peer_of(me, off):
    return ((me // 4 + off[0]) % 4) * 4 + (me % 4 + off[1]) % 4


def minus(off):
    return tuple((4 - o) % 4 for o in off)


def chip_core(me, dx, dc):
    return ((me // 2 + dx) % 4) * 2 + (me % 2 + dc) % 2


def cols(block):
    return pl.ds(pl.multiple_of(block * VD, VD), VD)


def rows_of(step, size):
    return pl.ds(pl.multiple_of(step * size, size), size)


def layer_kernel(
    q_ref, k_ref, v_ref, res_ref, lam_ref, gain_ref, ffn_ref, route_ref, weight_ref,
    wo_hbm, wg_hbm, wu_hbm, wd_hbm,
    out_ref,
    qa, ka, va, s1a, s2a, s1b, s2b, pbuf, obuf, att, mid, xin, onehot, chigh, clow,
    wo, wg, wu, wd, xs, rx, hid, yx, ret,
    ks, kr, vs, vr, qs, qr, os_, or_, ds, dr, es, er, lsem, wsem,
):
    sp = lax.axis_index("sp")
    dp = lax.axis_index("dp")
    expert = sp * 8 + dp
    barrier = pltpu.get_barrier_semaphore()

    def device(dx, off):
        return {"sp": peer_of(sp, off[:2]), "dp": chip_core(dp, dx, off[2])}

    for g in range(4):
        for j, off in enumerate(INNER):
            if (g, j) != (OWN_GROUP, OWN_AT):
                pl.semaphore_signal(
                    barrier, inc=1, device_id=device((2 - g) % 4, off), device_id_type=MESH
                )
    pl.semaphore_wait(barrier, 127)

    mine = cols(sp)
    sends = []
    for src, dst, ss, rs in ((k_ref, ka, ks, kr), (v_ref, va, vs, vr)):
        for i, off in enumerate(PEERS):
            to = peer_of(sp, off)
            copy = pltpu.make_async_remote_copy(
                src.at[:, cols(to)], dst.at[mine, :], ss.at[i], rs.at[i],
                device_id={"sp": to}, device_id_type=MESH,
            )
            copy.start()
            sends.append(copy)
        own = pltpu.make_async_copy(src.at[:, mine], dst.at[mine, :], rs.at[15])
        own.start()
        sends.append(own)

    def query_copy(i, b):
        to = 2 * ((sp // 2 + 8 - i) % 8) + b
        at = 2 * i + b
        return to, pltpu.make_async_remote_copy(
            q_ref.at[:, cols(to)], qa.at[mine, :], qs.at[at], qr.at[2 * i + sp % 2],
            device_id={"sp": to}, device_id_type=MESH,
        )

    for i in range(STEPS):
        for b in range(2):
            to, copy = query_copy(i, b)
            if i == 0:
                pl.when(to != sp)(copy.start)
            else:
                copy.start()
    own_query = pltpu.make_async_copy(q_ref.at[:, mine], qa.at[mine, :], qr.at[sp % 2])
    own_query.start()
    loads = []
    for i, (src, dst) in enumerate(((wo_hbm, wo), (wg_hbm, wg), (wu_hbm, wu), (wd_hbm, wd))):
        load = pltpu.make_async_copy(src, dst, wsem.at[i])
        load.start()
        loads.append(load)

    lanes = lax.broadcasted_iota(jnp.int32, (TOK, EXPERTS), 1)
    lower = (lax.broadcasted_iota(jnp.int32, (TOK, TOK), 0) > lax.broadcasted_iota(jnp.int32, (TOK, TOK), 1))
    lower = jnp.where(lower, 1.0, 0.0).astype(BF16)
    slot_lanes = lax.broadcasted_iota(jnp.int32, (TOK, SLOTS), 1).astype(F32)
    ahead = jnp.zeros((1, EXPERTS), F32)
    rows_mark = jnp.zeros((TOK, SLOTS), F32)
    combine = jnp.zeros((TOK, SLOTS), F32)
    for k in range(2):
        named = route_ref[:, k : k + 1]
        mark = jnp.where(named == lanes, 1.0, 0.0)
        before = jnp.dot(lower, mark.astype(BF16), preferred_element_type=F32) + ahead
        rank = jnp.sum(before * mark, axis=1, keepdims=True)
        slot = named.astype(F32) * CAP + rank
        here = slot == slot_lanes
        rows_mark = jnp.where(here, 1.0, rows_mark)
        combine = jnp.where(here, weight_ref[:, k : k + 1], combine)
        ahead = ahead + jnp.sum(mark, axis=0, keepdims=True)
    onehot[...] = rows_mark.astype(BF16)
    high = combine.astype(BF16)
    chigh[...] = high
    clow[...] = (combine - high.astype(F32)).astype(BF16)

    for copy in sends:
        if hasattr(copy, "wait_recv") and copy.is_remote:
            copy.wait_recv()
        else:
            copy.wait()

    lam = lam_ref[sp]
    gain = gain_ref[pl.ds(sp, 1), :] * 0.8
    first = lax.broadcasted_iota(jnp.int32, (QB, VD), 1) < HD
    scale = HD ** (-0.5) * LOG2E

    def pair_of(step):
        return (sp // 2 + step) % STEPS

    def queries_arrive(step):
        for b in range(2):
            pltpu.make_async_remote_copy(
                q_ref.at[:, mine], qa.at[cols(2 * pair_of(step) + b), :],
                qs.at[2 * step + b], qr.at[2 * step + b],
                device_id={"sp": sp}, device_id_type=MESH,
            ).wait_recv()

    def scores(step, s1, s2):
        q = qa[rows_of(pair_of(step), QB), :]
        zero = jnp.zeros_like(q)
        q1 = jnp.where(first, q, zero)
        q2 = jnp.where(first, zero, q)
        dims = (((1,), (1,)), ((), ()))
        for c in range(SEQ // KC):
            k = ka[c * KC : (c + 1) * KC, :]
            at = pl.ds(c * KC, KC)
            s1[:, at] = lax.dot_general(q1, k, dims, preferred_element_type=F32)
            s2[:, at] = lax.dot_general(q2, k, dims, preferred_element_type=F32)

    def mixed(step, s1, s2):
        inv = []
        for r in range(QB // RB):
            at = pl.ds(r * RB, RB)
            a = s1[at, :]
            e1 = jnp.exp2((a - jnp.max(a, axis=1, keepdims=True)) * scale)
            l1 = jnp.sum(e1, axis=1, keepdims=True)
            b = s2[at, :]
            e2 = jnp.exp2((b - jnp.max(b, axis=1, keepdims=True)) * scale)
            l2 = jnp.sum(e2, axis=1, keepdims=True)
            pbuf[at, :] = (e1 - e2 * (lam * l1 / l2)).astype(BF16)
            inv.append(1.0 / l1)
        out = jnp.dot(pbuf[...], va[...], preferred_element_type=F32)
        out = out * jnp.concatenate(inv, axis=0)
        out = out * lax.rsqrt(jnp.mean(out * out, axis=1, keepdims=True) + eps) * gain
        obuf[rows_of(pair_of(step), QB), :] = out.astype(BF16)

    def head_copy(to):
        return pltpu.make_async_remote_copy(
            obuf.at[cols(to), :], att.at[:, mine], os_.at[to], or_.at[sp],
            device_id={"sp": to}, device_id_type=MESH,
        )

    own_head = pltpu.make_async_copy(obuf.at[mine, :], att.at[:, mine], or_.at[sp])

    def heads_leave(step):
        for b in range(2):
            to = 2 * pair_of(step) + b
            pl.when(to != sp)(head_copy(to).start)
            pl.when(to == sp)(own_head.start)

    def pair(i, carry):
        step = 2 * i
        queries_arrive(step + 1)
        scores(step + 1, s1b, s2b)
        mixed(step, s1a, s2a)
        heads_leave(step)

        @pl.when(i < STEPS // 2 - 1)
        def _():
            queries_arrive(step + 2)

        scores((step + 2) % STEPS, s1a, s2a)
        mixed(step + 1, s1b, s2b)
        heads_leave(step + 1)
        return carry

    queries_arrive(0)
    scores(0, s1a, s2a)
    lax.fori_loop(0, STEPS // 2, pair, 0)

    for h in range(HEADS):
        pltpu.make_async_remote_copy(
            obuf.at[mine, :], att.at[:, h * VD : (h + 1) * VD], os_.at[h], or_.at[h],
            device_id={"sp": sp}, device_id_type=MESH,
        ).wait_recv()

    loads[0].wait()
    squares = jnp.zeros((TOK, 1), F32)
    for n in range(D // NC):
        at = slice(n * NC, (n + 1) * NC)
        projected = jnp.dot(att[...], wo[:, at], preferred_element_type=F32)
        whole = (res_ref[:, at].astype(F32) + projected).astype(BF16)
        mid[:, at] = whole
        whole = whole.astype(F32)
        squares = squares + jnp.sum(whole * whole, axis=1, keepdims=True)
    inverse = lax.rsqrt(squares * (1.0 / D) + eps)
    for n in range(D // NC):
        at = slice(n * NC, (n + 1) * NC)
        x = (mid[:, at].astype(F32) * inverse * ffn_ref[:, at]).astype(BF16)
        picked = lax.dot_general(
            onehot[...], x, (((0,), (0,)), ((), ())), preferred_element_type=F32
        ).astype(BF16)
        xs[:, :, at] = picked.reshape(EXPERTS, CAP, NC)

    for g in range(4):
        dx = (2 - g) % 4
        for j, off in enumerate(INNER):
            i = g * GROUP + j
            if (g, j) == (OWN_GROUP, OWN_AT):
                pltpu.make_async_copy(xs.at[expert], rx.at[i], dr.at[i]).start()
                continue
            to = device(dx, off)
            pltpu.make_async_remote_copy(
                xs.at[to["sp"] * 8 + to["dp"]], rx.at[i], ds.at[i], dr.at[i],
                device_id=to, device_id_type=MESH,
            ).start()
    for load in loads[1:]:
        load.wait()

    def dispatch_wait(i):
        return pltpu.make_async_remote_copy(
            xs.at[0], rx.at[i], ds.at[i], dr.at[i],
            device_id={"sp": sp}, device_id_type=MESH,
        )

    def batch(g, carry):
        at = rows_of(g, GROUP)
        for j in range(GROUP):
            dispatch_wait(g * GROUP + j).wait_recv()
        x = rx[at].reshape(GROUP * CAP, D)
        for n in range(FF // 256):
            w = slice(n * 256, (n + 1) * 256)
            gate = jnp.dot(x, wg[:, w], preferred_element_type=F32)
            up = jnp.dot(x, wu[:, w], preferred_element_type=F32)
            hid[:, w] = (gate / (1.0 + jnp.exp(-gate)) * up).astype(BF16)
        h = hid[...]
        for n in range(D // NC):
            w = slice(n * NC, (n + 1) * NC)
            y = jnp.dot(h, wd[:, w], preferred_element_type=F32).astype(BF16)
            yx[at, :, w] = y.reshape(GROUP, CAP, NC)
        dx = (g + 2) % 4
        for j, off in enumerate(INNER):
            i = g * GROUP + j
            back = pltpu.make_async_remote_copy(
                yx.at[i], ret.at[expert], es.at[i], er.at[i],
                device_id={
                    "sp": peer_of(sp, minus(off[:2])),
                    "dp": chip_core(dp, dx, off[2]),
                },
                device_id_type=MESH,
            )
            if j == OWN_AT:
                own = pltpu.make_async_copy(yx.at[i], ret.at[expert], er.at[i])
                pl.when(g != OWN_GROUP)(back.start)
                pl.when(g == OWN_GROUP)(own.start)
            else:
                back.start()
        return carry

    lax.fori_loop(0, 4, batch, 0)

    def returned(i):
        return pltpu.make_async_remote_copy(
            yx.at[i], ret.at[0], es.at[i], er.at[i],
            device_id={"sp": sp}, device_id_type=MESH,
        )

    for i in range(EXPERTS):
        returned(i).wait_recv()
    for n in range(D // NC):
        at = slice(n * NC, (n + 1) * NC)
        r = ret[:, :, at].reshape(SLOTS, NC)
        total = jnp.dot(chigh[...], r, preferred_element_type=F32)
        total = total + jnp.dot(clow[...], r, preferred_element_type=F32)
        out_ref[:, at] = (mid[:, at].astype(F32) + total).astype(BF16)

    for copy in sends:
        if copy.is_remote:
            copy.wait_send()
    for i in range(STEPS):
        for b in range(2):
            to, copy = query_copy(i, b)
            if i == 0:
                pl.when(to != sp)(copy.wait_send)
            else:
                copy.wait_send()
    for h in range(HEADS):
        pl.when(sp != h)(head_copy(h).wait_send)
    for i in range(EXPERTS):
        if i != OWN_GROUP * GROUP + OWN_AT:
            dispatch_wait(i).wait_send()
            returned(i).wait_send()


def on_device(
    residual, query_maps, key_maps, value_rows, lambdas, head_gain, out_weight, ffn_gain,
    routes, route_weights, expert_gate, expert_up, expert_down,
):
    vmem = pl.BlockSpec(memory_space=pltpu.VMEM)
    smem = pl.BlockSpec(memory_space=pltpu.SMEM)
    hbm = pl.BlockSpec(memory_space=pl.ANY)
    score = pltpu.VMEM((QB, SEQ), F32)
    rows = pltpu.VMEM((SEQ, VD), BF16)
    tokens = pltpu.VMEM((TOK, D), BF16)
    table = pltpu.VMEM((TOK, SLOTS), BF16)
    slots = pltpu.VMEM((EXPERTS, CAP, D), BF16)
    sem = pltpu.SemaphoreType.DMA
    out = pl.pallas_call(
        layer_kernel,
        out_shape=jax.ShapeDtypeStruct((TOK, D), BF16),
        in_specs=[vmem] * 4 + [smem] + [vmem] * 4 + [hbm] * 4,
        out_specs=vmem,
        scratch_shapes=[rows, rows, rows, score, score, score, score,
                        pltpu.VMEM((QB, SEQ), BF16), rows, tokens, tokens, tokens,
                        table, table, table,
                        pltpu.VMEM((D, D), BF16), pltpu.VMEM((D, FF), BF16),
                        pltpu.VMEM((D, FF), BF16), pltpu.VMEM((FF, D), BF16),
                        slots, slots, pltpu.VMEM((GROUP * CAP, FF), BF16), slots, slots]
        + [sem((16,))] * 8 + [sem((EXPERTS,))] * 4 + [sem((4,))] * 2,
        compiler_params=pltpu.CompilerParams(
            collective_id=0, has_side_effects=True, vmem_limit_bytes=60 * 2**20
        ),
        name="layer",
    )(
        query_maps[0], key_maps[0], value_rows[0], residual[0], lambdas,
        head_gain.reshape(HEADS, VD), ffn_gain.reshape(1, D), routes[0], route_weights[0],
        out_weight, expert_gate[0], expert_up[0], expert_down[0],
    )
    return out[None]


def solution(mesh):
    tokens = P("dp", "sp", None)
    experts = P(("sp", "dp"), None, None)
    placed = (tokens,) * 4 + (P(),) * 4 + (tokens,) * 2 + (experts,) * 3
    return jax.shard_map(
        on_device, mesh=mesh, in_specs=placed, out_specs=tokens, check_vma=False
    )
```

time: 175 us -> 119 us (0.68)
  Pallas kernels: 49.9 us -> 115 us
  blocking collectives: 38.6 us -> 0 us
  waiting for transfers between devices: 30.5 us -> 0 us
  matrix products: 20.7 us -> 0 us
  local copies, waits for them, and re-layouts: 24.4 us -> 4.7 us
  other arithmetic: 5.41 us -> 0 us
  starting transfers between devices: 4.55 us -> 0 us
    pallas_call x1, Pallas kernels: 49.9 us -> 115 us  [on_device(): pl.pallas_call(layer_kernel, out_shape=jax.ShapeDtypeStruct((TOK, D), BF1...]
    all_to_all x1 -> x0, blocking collectives: 38.6 us -> none  [exchange_both(): lax.all_to_all(blocks, axis, split_axis=0, concat_axis=0, tiled=True)]
    all_to_all x1 -> x0, waiting for transfers between devices: 30.5 us -> none  [exchange_both(): lax.all_to_all(blocks, axis, split_axis=0, concat_axis=0, tiled=True)]
    dot_general x3 -> x0, matrix products: 20.7 us -> none  [the longest x1 9.95 us: on_device(): jnp.dot(hidden, expert_down[0], preferred_element_type=jnp.float32)]
    another operation x7 -> x0, local copies, waits for them, and re-layouts: 11.9 us -> none  [the longest x2 6.85 us: exchange_both(): blocks = blocks.reshape(-1, *inside)]
    gather x2 -> x0, local copies, waits for them, and re-layouts: 5.7 us -> none  [the longest x1 3.35 us: on_device(): buffer = padded_input[slot_token].reshape(experts_all, capacity, D)]
    all_to_all x1 -> x0, starting transfers between devices: 4.55 us -> none  [exchange_both(): lax.all_to_all(blocks, axis, split_axis=0, concat_axis=0, tiled=True)]
    reduce_sum x2 -> x0, other arithmetic: 3.35 us -> none  [the longest x1 3.16 us: on_device(): layer_out = (middle + jnp.sum(weighted, axis=1)).astype(jnp.bfloat16)]
  transfers between devices with their start and end apart: 1 -> 0, of which waited for: 1 -> 0; matrix products, arithmetic and copies ran while one was open for 0% -> 0% of each run, Pallas kernels for 0% -> 0%
where the time goes in v2:
time: 119 us
  Pallas kernels  115 us (97%)
  local copies, waits for them, and re-layouts  4.7 us (4%)
    pallas_call x1, Pallas kernels, on_device(): pl.pallas_call(layer_kernel, out_shape=jax.ShapeDtypeStruct((TOK, D), BF1...  115 us
    unnamed x3, local copies, waits for them, and re-layouts  4.7 us

profile of v2, /device:TPU:1, one launch (start us, length us, event | category | flops | bytes accessed | tf_op | source)
XLA Modules:
  0.0 119.2 jit_solution(11615255984920020372)
XLA Ops:
  0.0 1.4 %copy.14 = s32[1,128,2]{2,1,0:T(8,128)} copy(s32[1,128,2]{1,2,0:T(2,128)} %param.21) | data formatting | bytes 2048 | tf_op args[8]
  1.4 1.4 %copy.15 = f32[1,128,2]{2,1,0:T(8,128)} copy(f32[1,128,2]{1,2,0:T(2,128)} %param.22) | data formatting | bytes 2048 | tf_op args[9]
  2.8 114.5 %layer.1 = bf16[128,2048]{1,0:T(8,128)(2,1)} custom-call(bf16[128,2048]{1,0:T(8,128)(2,1)} %bitcast.16, bf16[128,2048]{1,0:T(8,128)(2,1)} %bitcast.17, bf16[128,2048]{1,0:T(8,128)(2,1)} %bitcast.18, bf16[128,2048]{1,0:T(8,128)(2,1)} %bitcast.19, f32[16]{0:T(128)} %lam_ref.1, f32[16,128]{1,0:T(8,128)} %bitcast.22, f32[1,2048]{1,0:T(1,128)} %bitcast.23, ...), custom_call_target="tpu_custom_call" | custom-call | tf_op jit(solution)/shard_map/layer/pallas_call | solution.py:354
  117.4 1.9 %copy.17 = bf16[1,128,2048]{2,1,0:T(8,128)(2,1)} copy(bf16[1,128,2048]{2,1,0:T(8,128)(2,1)} %bitcast.15) | data formatting | bytes 1048576

commit v3 on v2

v3 whole, which is shorter than its diff:
```python
import jax
import jax.numpy as jnp
from jax import lax
from jax.experimental import pallas as pl
from jax.experimental.pallas import tpu as pltpu
from jax.sharding import PartitionSpec as P

D = 2048
HEADS = 16
HD = 64
VD = 128
FF = 1024
TOK = 128
SEQ = 2048
EXPERTS = 128
CAP = 4
SLOTS = EXPERTS * CAP
QB = 256
STEPS = SEQ // QB
KC = 256
RB = 16
NC = 512
GROUP = 32
MESH = pl.DeviceIdType.MESH
eps = 1e-06
LOG2E = 1.4426950408889634
F32 = jnp.float32
BF16 = jnp.bfloat16
NEAR = {0: 0, 1: 1, 2: 2, 3: 1}
PEERS = sorted(
    [(a, b) for a in range(4) for b in range(4) if (a, b) != (0, 0)],
    key=lambda o: -(NEAR[o[0]] + NEAR[o[1]]),
)
INNER = [(a, b, c) for a, b in PEERS + [(0, 0)] for c in (1, 0)]
OWN_GROUP, OWN_AT = 0, INNER.index((0, 0, 0))


def peer_of(me, off):
    return ((me // 4 + off[0]) % 4) * 4 + (me % 4 + off[1]) % 4


def minus(off):
    return tuple((4 - o) % 4 for o in off)


def chip_core(me, dx, dc):
    return ((me // 2 + dx) % 4) * 2 + (me % 2 + dc) % 2


def cols(block):
    return pl.ds(pl.multiple_of(block * VD, VD), VD)


def rows_of(step, size):
    return pl.ds(pl.multiple_of(step * size, size), size)


def layer_kernel(
    q_hbm, k_hbm, v_hbm, res_hbm, lam_ref, gain_ref, ffn_ref, route_ref, weight_ref,
    wo_hbm, wg_hbm, wu_hbm, wd_hbm,
    out_ref,
    q_ref, k_ref, v_ref, res_ref,
    qa, ka, va, s1a, s2a, s1b, s2b, pbuf, obuf, att, mid, onehot, chigh, clow,
    wo, wg, wu, wd, xs, rx, hid, yx, ret,
    kvs, kvr, qs, qr, os_, or_, ds, dr, es, er, insem, wsem, ready,
):
    sp = lax.axis_index("sp")
    dp = lax.axis_index("dp")
    expert = sp * 8 + dp
    barrier = pltpu.get_barrier_semaphore()
    for off in PEERS:
        pl.semaphore_signal(barrier, inc=1, device_id={"sp": peer_of(sp, off)}, device_id_type=MESH)
    for i in range(1, 8):
        to = chip_core(dp, i // 2, i % 2)
        pl.semaphore_signal(barrier, inc=1, device_id={"dp": to}, device_id_type=MESH)
    inputs = []
    for i, (src, dst) in enumerate(((k_hbm, k_ref), (v_hbm, v_ref), (q_hbm, q_ref), (res_hbm, res_ref))):
        load = pltpu.make_async_copy(src, dst, insem.at[i])
        load.start()
        inputs.append(load)
    pl.semaphore_wait(barrier, 22)
    for off in PEERS:
        pl.semaphore_signal(ready, inc=1, device_id={"sp": peer_of(sp, off)}, device_id_type=MESH)

    mine = cols(sp)
    for n, (src, dst) in enumerate(((k_ref, ka), (v_ref, va))):
        inputs[n].wait()
        for off in PEERS:
            to = peer_of(sp, off)
            pltpu.make_async_remote_copy(
                src.at[:, cols(to)], dst.at[mine, :], kvs.at[n], kvr.at[n],
                device_id={"sp": to}, device_id_type=MESH,
            ).start()
        pltpu.make_async_copy(src.at[:, mine], dst.at[mine, :], kvr.at[n]).start()

    def query_copy(i, b):
        to = 2 * ((sp // 2 + 8 - i) % 8) + b
        return to, pltpu.make_async_remote_copy(
            q_ref.at[:, cols(to)], qa.at[mine, :], qs.at[2 * i + b], qr.at[2 * i + sp % 2],
            device_id={"sp": to}, device_id_type=MESH,
        )

    inputs[2].wait()
    pltpu.make_async_copy(q_ref.at[:, mine], qa.at[mine, :], qr.at[sp % 2]).start()
    for i in range(STEPS):
        for b in range(2):
            to, copy = query_copy(i, b)
            if i == 0:
                pl.when(to != sp)(copy.start)
            else:
                copy.start()
    loads = []
    for i, (src, dst) in enumerate(((wo_hbm, wo), (wg_hbm, wg), (wu_hbm, wu), (wd_hbm, wd))):
        load = pltpu.make_async_copy(src, dst, wsem.at[i])
        load.start()
        loads.append(load)

    names = lax.broadcasted_iota(jnp.int32, (EXPERTS, TOK), 0)
    earlier = lax.broadcasted_iota(jnp.int32, (TOK, TOK), 0) < lax.broadcasted_iota(jnp.int32, (TOK, TOK), 1)
    earlier = jnp.where(earlier, 1.0, 0.0).astype(BF16)
    slots = lax.broadcasted_iota(jnp.int32, (SLOTS, TOK), 0).astype(F32)
    ahead = jnp.zeros((EXPERTS, 1), F32)
    marks = jnp.zeros((SLOTS, TOK), F32)
    combine = jnp.zeros((SLOTS, TOK), F32)
    for k in range(2):
        named = route_ref[k : k + 1, :]
        mark = jnp.where(named == names, 1.0, 0.0)
        before = jnp.dot(mark.astype(BF16), earlier, preferred_element_type=F32) + ahead
        rank = jnp.sum(before * mark, axis=0, keepdims=True)
        here = named.astype(F32) * CAP + rank == slots
        marks = jnp.where(here, 1.0, marks)
        combine = jnp.where(here, weight_ref[k : k + 1, :], combine)
        ahead = ahead + jnp.sum(mark, axis=1, keepdims=True)
    onehot[...] = marks.astype(BF16)
    high = combine.astype(BF16)
    chigh[...] = high
    clow[...] = (combine - high.astype(F32)).astype(BF16)

    def all_blocks(src, dst, ss, rs, count):
        size = src.shape[0] // 16 * count
        return pltpu.make_async_remote_copy(
            src.at[pl.ds(0, size)], dst.at[pl.ds(0, size)], ss, rs,
            device_id={"sp": sp}, device_id_type=MESH,
        )

    all_blocks(ka, ka, kvs.at[0], kvr.at[0], 16).wait_recv()
    all_blocks(va, va, kvs.at[1], kvr.at[1], 16).wait_recv()

    lam = lam_ref[sp]
    gain = gain_ref[pl.ds(sp, 1), :] * 0.8
    first = lax.broadcasted_iota(jnp.int32, (QB, VD), 1) < HD
    scale = HD ** (-0.5) * LOG2E

    def pair_of(step):
        return (sp // 2 + step) % STEPS

    def queries_arrive(step):
        for b in range(2):
            pltpu.make_async_remote_copy(
                q_ref.at[:, mine], qa.at[cols(2 * pair_of(step) + b), :],
                qs.at[2 * step + b], qr.at[2 * step + b],
                device_id={"sp": sp}, device_id_type=MESH,
            ).wait_recv()

    def scores(step, s1, s2):
        q = qa[rows_of(pair_of(step), QB), :]
        zero = jnp.zeros_like(q)
        q1 = jnp.where(first, q, zero)
        q2 = jnp.where(first, zero, q)
        dims = (((1,), (1,)), ((), ()))
        for c in range(SEQ // KC):
            k = ka[c * KC : (c + 1) * KC, :]
            at = pl.ds(c * KC, KC)
            s1[:, at] = lax.dot_general(q1, k, dims, preferred_element_type=F32)
            s2[:, at] = lax.dot_general(q2, k, dims, preferred_element_type=F32)

    def mixed(step, s1, s2):
        inv = []
        for r in range(QB // RB):
            at = pl.ds(r * RB, RB)
            a = s1[at, :]
            e1 = jnp.exp2((a - jnp.max(a, axis=1, keepdims=True)) * scale)
            l1 = jnp.sum(e1, axis=1, keepdims=True)
            b = s2[at, :]
            e2 = jnp.exp2((b - jnp.max(b, axis=1, keepdims=True)) * scale)
            l2 = jnp.sum(e2, axis=1, keepdims=True)
            pbuf[at, :] = (e1 - e2 * (lam * l1 / l2)).astype(BF16)
            inv.append(1.0 / l1)
        out = jnp.dot(pbuf[...], va[...], preferred_element_type=F32)
        out = out * jnp.concatenate(inv, axis=0)
        out = out * lax.rsqrt(jnp.mean(out * out, axis=1, keepdims=True) + eps) * gain
        obuf[rows_of(pair_of(step), QB), :] = out.astype(BF16)

    def head_copy(to):
        return pltpu.make_async_remote_copy(
            obuf.at[cols(to), :], att.at[:, mine], os_, or_,
            device_id={"sp": to}, device_id_type=MESH,
        )

    own_head = pltpu.make_async_copy(obuf.at[mine, :], att.at[:, mine], or_)

    def heads_leave(step):
        for b in range(2):
            to = 2 * pair_of(step) + b
            pl.when(to != sp)(head_copy(to).start)
            pl.when(to == sp)(own_head.start)

    def pair(i, carry):
        step = 2 * i
        queries_arrive(step + 1)
        scores(step + 1, s1b, s2b)
        mixed(step, s1a, s2a)
        heads_leave(step)

        @pl.when(i < STEPS // 2 - 1)
        def _():
            queries_arrive(step + 2)

        scores((step + 2) % STEPS, s1a, s2a)
        mixed(step + 1, s1b, s2b)
        heads_leave(step + 1)
        return carry

    queries_arrive(0)
    scores(0, s1a, s2a)
    lax.fori_loop(0, STEPS // 2, pair, 0)

    inputs[3].wait()
    loads[0].wait()
    all_blocks(obuf, obuf, os_, or_, 16).wait_recv()

    squares = jnp.zeros((TOK, 1), F32)
    for n in range(D // NC):
        at = slice(n * NC, (n + 1) * NC)
        projected = jnp.dot(att[...], wo[:, at], preferred_element_type=F32)
        whole = (res_ref[:, at].astype(F32) + projected).astype(BF16)
        mid[:, at] = whole
        whole = whole.astype(F32)
        squares = squares + jnp.sum(whole * whole, axis=1, keepdims=True)
    inverse = lax.rsqrt(squares * (1.0 / D) + eps)
    for n in range(D // NC):
        at = slice(n * NC, (n + 1) * NC)
        x = (mid[:, at].astype(F32) * inverse * ffn_ref[:, at]).astype(BF16)
        picked = jnp.dot(onehot[...], x, preferred_element_type=F32).astype(BF16)
        xs[:, :, at] = picked.reshape(EXPERTS, CAP, NC)

    pl.semaphore_wait(ready, 15)
    peers = [peer_of(sp, off) for off in PEERS] + [sp]
    others = [[chip_core(dp, dx, dc) for dc in range(2)] for dx in range(4)]
    for g in range(4):
        for j, (dz, dy, dc) in enumerate(INNER):
            i = g * GROUP + j
            if (g, j) == (OWN_GROUP, OWN_AT):
                pltpu.make_async_copy(xs.at[expert], rx.at[i], dr.at[g]).start()
                continue
            to_sp, to_dp = peers[j // 2], others[(g + dz + dy) % 4][dc]
            pltpu.make_async_remote_copy(
                xs.at[to_sp * 8 + to_dp], rx.at[i], ds.at[g], dr.at[g],
                device_id={"sp": to_sp, "dp": to_dp}, device_id_type=MESH,
            ).start()
    for load in loads[1:]:
        load.wait()

    def whole_batch(src, dst, ss, rs, count):
        return pltpu.make_async_remote_copy(
            src.at[pl.ds(0, count)], dst.at[pl.ds(0, count)], ss, rs,
            device_id={"sp": sp}, device_id_type=MESH,
        )

    homes = [peer_of(sp, minus(off)) for off in PEERS] + [sp]

    def batch(g, carry):
        at = rows_of(g, GROUP)
        whole_batch(xs, rx, ds.at[g], dr.at[g], GROUP).wait_recv()
        x = rx[at].reshape(GROUP * CAP, D)
        for n in range(FF // 256):
            w = slice(n * 256, (n + 1) * 256)
            gate = jnp.dot(x, wg[:, w], preferred_element_type=F32)
            up = jnp.dot(x, wu[:, w], preferred_element_type=F32)
            hid[:, w] = (gate / (1.0 + jnp.exp(-gate)) * up).astype(BF16)
        h = hid[...]
        for n in range(D // NC):
            w = slice(n * NC, (n + 1) * NC)
            y = jnp.dot(h, wd[:, w], preferred_element_type=F32).astype(BF16)
            yx[at, :, w] = y.reshape(GROUP, CAP, NC)
        back_to = [[chip_core(dp, (8 - g - turn) % 4, dc) for dc in range(2)] for turn in range(4)]
        for j, (dz, dy, dc) in enumerate(INNER):
            i = g * GROUP + j
            back = pltpu.make_async_remote_copy(
                yx.at[i], ret.at[expert], es.at[g], er.at[g],
                device_id={"sp": homes[j // 2], "dp": back_to[(dz + dy) % 4][dc]},
                device_id_type=MESH,
            )
            if j == OWN_AT:
                own = pltpu.make_async_copy(yx.at[i], ret.at[expert], er.at[g])
                pl.when(g != OWN_GROUP)(back.start)
                pl.when(g == OWN_GROUP)(own.start)
            else:
                back.start()
        return carry

    lax.fori_loop(0, 4, batch, 0)

    for g in range(4):
        whole_batch(yx, ret, es.at[g], er.at[g], GROUP).wait_recv()
    for n in range(D // NC):
        at = slice(n * NC, (n + 1) * NC)
        r = ret[:, :, at].reshape(SLOTS, NC)
        dims = (((0,), (0,)), ((), ()))
        total = lax.dot_general(chigh[...], r, dims, preferred_element_type=F32)
        total = total + lax.dot_general(clow[...], r, dims, preferred_element_type=F32)
        out_ref[:, at] = (mid[:, at].astype(F32) + total).astype(BF16)

    all_blocks(ka, ka, kvs.at[0], kvr.at[0], 15).wait_send()
    all_blocks(va, va, kvs.at[1], kvr.at[1], 15).wait_send()
    all_blocks(obuf, obuf, os_, or_, 15).wait_send()
    for g in range(4):
        count = GROUP - (g == OWN_GROUP)
        whole_batch(xs, rx, ds.at[g], dr.at[g], count).wait_send()
        whole_batch(yx, ret, es.at[g], er.at[g], count).wait_send()
    for i in range(STEPS):
        for b in range(2):
            to, copy = query_copy(i, b)
            if i == 0:
                pl.when(to != sp)(copy.wait_send)
            else:
                copy.wait_send()


def on_device(
    residual, query_maps, key_maps, value_rows, lambdas, head_gain, out_weight, ffn_gain,
    routes, route_weights, expert_gate, expert_up, expert_down,
):
    vmem = pl.BlockSpec(memory_space=pltpu.VMEM)
    smem = pl.BlockSpec(memory_space=pltpu.SMEM)
    hbm = pl.BlockSpec(memory_space=pl.ANY)
    score = pltpu.VMEM((QB, SEQ), F32)
    rows = pltpu.VMEM((SEQ, VD), BF16)
    tokens = pltpu.VMEM((TOK, D), BF16)
    table = pltpu.VMEM((SLOTS, TOK), BF16)
    slots = pltpu.VMEM((EXPERTS, CAP, D), BF16)
    sem = pltpu.SemaphoreType.DMA
    out = pl.pallas_call(
        layer_kernel,
        out_shape=jax.ShapeDtypeStruct((TOK, D), BF16),
        in_specs=[hbm] * 4 + [smem] + [vmem] * 4 + [hbm] * 4,
        out_specs=vmem,
        scratch_shapes=[tokens] * 4 + [rows, rows, rows, score, score, score, score,
                        pltpu.VMEM((QB, SEQ), BF16), rows, tokens, tokens,
                        table, table, table,
                        pltpu.VMEM((D, D), BF16), pltpu.VMEM((D, FF), BF16),
                        pltpu.VMEM((D, FF), BF16), pltpu.VMEM((FF, D), BF16),
                        slots, slots, pltpu.VMEM((GROUP * CAP, FF), BF16), slots, slots]
        + [sem((2,)), sem((2,)), sem((16,)), sem((16,)), sem, sem] + [sem((4,))] * 6
        + [pltpu.SemaphoreType.REGULAR],
        compiler_params=pltpu.CompilerParams(
            collective_id=0, has_side_effects=True, vmem_limit_bytes=60 * 2**20
        ),
        name="layer",
    )(
        query_maps[0], key_maps[0], value_rows[0], residual[0], lambdas,
        head_gain.reshape(HEADS, VD), ffn_gain.reshape(1, D), routes[0].T, route_weights[0].T,
        out_weight, expert_gate[0], expert_up[0], expert_down[0],
    )
    return out[None]


def solution(mesh):
    tokens = P("dp", "sp", None)
    experts = P(("sp", "dp"), None, None)
    placed = (tokens,) * 4 + (P(),) * 4 + (tokens,) * 2 + (experts,) * 3
    return jax.shard_map(
        on_device, mesh=mesh, in_specs=placed, out_specs=tokens, check_vma=False
    )
```

time: 119 us -> 98.2 us (0.83); the launches traced: 119 us -> 96.6 us
  Pallas kernels: 115 us -> 94.8 us
  local copies, waits for them, and re-layouts: 4.7 us -> 1.88 us
    pallas_call x1, Pallas kernels: 115 us -> 94.8 us  [on_device(): pl.pallas_call(layer_kernel, out_shape=jax.ShapeDtypeStruct((TOK, D), BF1...]
    unnamed x3 -> x1, local copies, waits for them, and re-layouts: 4.7 us -> 1.88 us
where the time goes in v3:
time: 98.2 us; the launch traced here: 96.6 us
  Pallas kernels  94.8 us (97%)
  local copies, waits for them, and re-layouts  1.88 us (2%)
    pallas_call x1, Pallas kernels, on_device(): pl.pallas_call(layer_kernel, out_shape=jax.ShapeDtypeStruct((TOK, D), BF1...  94.8 us

profile of v3, /device:TPU:1, one launch (start us, length us, event | category | flops | bytes accessed | tf_op | source)
XLA Modules:
  0.0 96.6 jit_solution(11713173143535698481)
XLA Ops:
  0.0 94.8 %layer.1 = bf16[128,2048]{1,0:T(8,128)(2,1)} custom-call(bf16[128,2048]{1,0:T(8,128)(2,1)} %bitcast.20, bf16[128,2048]{1,0:T(8,128)(2,1)} %bitcast.21, bf16[128,2048]{1,0:T(8,128)(2,1)} %bitcast.22, bf16[128,2048]{1,0:T(8,128)(2,1)} %bitcast.23, f32[16]{0:T(128)} %lam_ref.1, f32[16,128]{1,0:T(8,128)} %bitcast.24, f32[1,2048]{1,0:T(1,128)} %bitcast.25, ...), custom_call_target="tpu_custom_call" | custom-call | tf_op jit(solution)/shard_map/layer/pallas_call | solution.py:343
  94.8 1.9 %copy.15 = bf16[1,128,2048]{2,1,0:T(8,128)(2,1)} copy(bf16[1,128,2048]{2,1,0:T(8,128)(2,1)} %bitcast.19) | data formatting | bytes 1048576

commit v4 on v3

--- a/solution.py
+++ b/solution.py
@@ -17,6 +17,7 @@
 SLOTS = EXPERTS * CAP
 QB = 256
 STEPS = SEQ // QB
+HALF = STEPS // 2
 KC = 256
 RB = 16
 NC = 512
@@ -58,11 +59,11 @@
 def layer_kernel(
     q_hbm, k_hbm, v_hbm, res_hbm, lam_ref, gain_ref, ffn_ref, route_ref, weight_ref,
     wo_hbm, wg_hbm, wu_hbm, wd_hbm,
-    out_ref,
+    out_hbm,
     q_ref, k_ref, v_ref, res_ref,
-    qa, ka, va, s1a, s2a, s1b, s2b, pbuf, obuf, att, mid, onehot, chigh, clow,
+    qa, ka, va, s1a, s2a, s1b, s2b, maps, sums, obuf, att, total, mid, out, onehot, chigh, clow,
     wo, wg, wu, wd, xs, rx, hid, yx, ret,
-    kvs, kvr, qs, qr, os_, or_, ds, dr, es, er, insem, wsem, ready,
+    kvs, kvr, qs, qr, os_, or_, ds, dr, es, er, insem, wsem, outsem, ready,
 ):
     sp = lax.axis_index("sp")
     dp = lax.axis_index("dp")
@@ -83,7 +84,8 @@
         pl.semaphore_signal(ready, inc=1, device_id={"sp": peer_of(sp, off)}, device_id_type=MESH)
 
     mine = cols(sp)
-    for n, (src, dst) in enumerate(((k_ref, ka), (v_ref, va))):
+
+    def rows_leave(n, src, dst):
         inputs[n].wait()
         for off in PEERS:
             to = peer_of(sp, off)
@@ -100,15 +102,21 @@
             device_id={"sp": to}, device_id_type=MESH,
         )
 
+    def queries_leave(steps):
+        for i in steps:
+            for b in range(2):
+                to, copy = query_copy(i, b)
+                if i == 0:
+                    pl.when(to != sp)(copy.start)
+                else:
+                    copy.start()
+
+    rows_leave(0, k_ref, ka)
     inputs[2].wait()
     pltpu.make_async_copy(q_ref.at[:, mine], qa.at[mine, :], qr.at[sp % 2]).start()
-    for i in range(STEPS):
-        for b in range(2):
-            to, copy = query_copy(i, b)
-            if i == 0:
-                pl.when(to != sp)(copy.start)
-            else:
-                copy.start()
+    queries_leave(range(HALF))
+    rows_leave(1, v_ref, va)
+    queries_leave(range(HALF, STEPS))
     loads = []
     for i, (src, dst) in enumerate(((wo_hbm, wo), (wg_hbm, wg), (wu_hbm, wu), (wd_hbm, wd))):
         load = pltpu.make_async_copy(src, dst, wsem.at[i])
@@ -144,7 +152,6 @@
         )
 
     all_blocks(ka, ka, kvs.at[0], kvr.at[0], 16).wait_recv()
-    all_blocks(va, va, kvs.at[1], kvr.at[1], 16).wait_recv()
 
     lam = lam_ref[sp]
     gain = gain_ref[pl.ds(sp, 1), :] * 0.8
@@ -175,7 +182,6 @@
             s2[:, at] = lax.dot_general(q2, k, dims, preferred_element_type=F32)
 
     def mixed(step, s1, s2):
-        inv = []
         for r in range(QB // RB):
             at = pl.ds(r * RB, RB)
             a = s1[at, :]
@@ -184,56 +190,67 @@
             b = s2[at, :]
             e2 = jnp.exp2((b - jnp.max(b, axis=1, keepdims=True)) * scale)
             l2 = jnp.sum(e2, axis=1, keepdims=True)
-            pbuf[at, :] = (e1 - e2 * (lam * l1 / l2)).astype(BF16)
-            inv.append(1.0 / l1)
-        out = jnp.dot(pbuf[...], va[...], preferred_element_type=F32)
-        out = out * jnp.concatenate(inv, axis=0)
+            maps[step, at, :] = (e1 - e2 * (lam * l1 / l2)).astype(BF16)
+            sums[step, at, :] = l1
+
+    def valued(step):
+        out = jnp.dot(maps[step], va[...], preferred_element_type=F32)
+        out = out / sums[step]
         out = out * lax.rsqrt(jnp.mean(out * out, axis=1, keepdims=True) + eps) * gain
         obuf[rows_of(pair_of(step), QB), :] = out.astype(BF16)
-
-    def head_copy(to):
-        return pltpu.make_async_remote_copy(
-            obuf.at[cols(to), :], att.at[:, mine], os_, or_,
-            device_id={"sp": to}, device_id_type=MESH,
-        )
-
-    own_head = pltpu.make_async_copy(obuf.at[mine, :], att.at[:, mine], or_)
 
     def heads_leave(step):
         for b in range(2):
             to = 2 * pair_of(step) + b
-            pl.when(to != sp)(head_copy(to).start)
-            pl.when(to == sp)(own_head.start)
+            copy = pltpu.make_async_remote_copy(
+                obuf.at[cols(to), :], att.at[:, mine], os_, or_.at[step],
+                device_id={"sp": to}, device_id_type=MESH,
+            )
+            if step:
+                copy.start()
+            else:
+                own = pltpu.make_async_copy(obuf.at[mine, :], att.at[:, mine], or_.at[0])
+                pl.when(to != sp)(copy.start)
+                pl.when(to == sp)(own.start)
 
     def pair(i, carry):
         step = 2 * i
         queries_arrive(step + 1)
         scores(step + 1, s1b, s2b)
         mixed(step, s1a, s2a)
-        heads_leave(step)
-
-        @pl.when(i < STEPS // 2 - 1)
-        def _():
-            queries_arrive(step + 2)
-
-        scores((step + 2) % STEPS, s1a, s2a)
+        queries_arrive(step + 2)
+        scores(step + 2, s1a, s2a)
         mixed(step + 1, s1b, s2b)
-        heads_leave(step + 1)
         return carry
 
     queries_arrive(0)
     scores(0, s1a, s2a)
-    lax.fori_loop(0, STEPS // 2, pair, 0)
+    lax.fori_loop(0, HALF // 2, pair, 0)
+    all_blocks(va, va, kvs.at[1], kvr.at[1], 16).wait_recv()
+    for step in range(HALF, STEPS):
+        now, later = ((s1a, s2a), (s1b, s2b))[:: 1 if step % 2 == 0 else -1]
+        if step + 1 < STEPS:
+            queries_arrive(step + 1)
+            scores(step + 1, *later)
+        mixed(step, *now)
+        for done in (2 * (step - HALF), 2 * (step - HALF) + 1):
+            valued(done)
+            heads_leave(done)
 
     inputs[3].wait()
     loads[0].wait()
-    all_blocks(obuf, obuf, os_, or_, 16).wait_recv()
+    for step in range(STEPS):
+        all_blocks(obuf, obuf, os_, or_.at[step], 2).wait_recv()
+        heads = rows_of((sp // 2 + STEPS - step) % STEPS, 2 * VD)
+        for n in range(D // NC):
+            at = slice(n * NC, (n + 1) * NC)
+            part = jnp.dot(att[:, heads], wo[heads, at], preferred_element_type=F32)
+            total[:, at] = part + total[:, at] if step else part
 
     squares = jnp.zeros((TOK, 1), F32)
     for n in range(D // NC):
         at = slice(n * NC, (n + 1) * NC)
-        projected = jnp.dot(att[...], wo[:, at], preferred_element_type=F32)
-        whole = (res_ref[:, at].astype(F32) + projected).astype(BF16)
+        whole = (res_ref[:, at].astype(F32) + total[:, at]).astype(BF16)
         mid[:, at] = whole
         whole = whole.astype(F32)
         squares = squares + jnp.sum(whole * whole, axis=1, keepdims=True)
@@ -303,13 +320,17 @@
 
     for g in range(4):
         whole_batch(yx, ret, es.at[g], er.at[g], GROUP).wait_recv()
+    leaving = []
     for n in range(D // NC):
         at = slice(n * NC, (n + 1) * NC)
         r = ret[:, :, at].reshape(SLOTS, NC)
         dims = (((0,), (0,)), ((), ()))
-        total = lax.dot_general(chigh[...], r, dims, preferred_element_type=F32)
-        total = total + lax.dot_general(clow[...], r, dims, preferred_element_type=F32)
-        out_ref[:, at] = (mid[:, at].astype(F32) + total).astype(BF16)
+        moe = lax.dot_general(chigh[...], r, dims, preferred_element_type=F32)
+        moe = moe + lax.dot_general(clow[...], r, dims, preferred_element_type=F32)
+        out[:, at] = (mid[:, at].astype(F32) + moe).astype(BF16)
+        leave = pltpu.make_async_copy(out.at[:, at], out_hbm.at[:, at], outsem.at[n])
+        leave.start()
+        leaving.append(leave)
 
     all_blocks(ka, ka, kvs.at[0], kvr.at[0], 15).wait_send()
     all_blocks(va, va, kvs.at[1], kvr.at[1], 15).wait_send()
@@ -325,6 +346,8 @@
                 pl.when(to != sp)(copy.wait_send)
             else:
                 copy.wait_send()
+    for leave in leaving:
+        leave.wait()
 
 
 def on_device(
@@ -344,14 +367,15 @@
         layer_kernel,
         out_shape=jax.ShapeDtypeStruct((TOK, D), BF16),
         in_specs=[hbm] * 4 + [smem] + [vmem] * 4 + [hbm] * 4,
-        out_specs=vmem,
+        out_specs=hbm,
         scratch_shapes=[tokens] * 4 + [rows, rows, rows, score, score, score, score,
-                        pltpu.VMEM((QB, SEQ), BF16), rows, tokens, tokens,
+                        pltpu.VMEM((STEPS, QB, SEQ), BF16), pltpu.VMEM((STEPS, QB, 1), F32), rows, tokens,
+                        pltpu.VMEM((TOK, D), F32), tokens, tokens,
                         table, table, table,
                         pltpu.VMEM((D, D), BF16), pltpu.VMEM((D, FF), BF16),
                         pltpu.VMEM((D, FF), BF16), pltpu.VMEM((FF, D), BF16),
                         slots, slots, pltpu.VMEM((GROUP * CAP, FF), BF16), slots, slots]
-        + [sem((2,)), sem((2,)), sem((16,)), sem((16,)), sem, sem] + [sem((4,))] * 6
+        + [sem((2,)), sem((2,)), sem((16,)), sem((16,)), sem, sem((STEPS,))] + [sem((4,))] * 7
         + [pltpu.SemaphoreType.REGULAR],
         compiler_params=pltpu.CompilerParams(
             collective_id=0, has_side_effects=True, vmem_limit_bytes=60 * 2**20

time: 98.2 us -> 97.9 us (level); the launches traced: 96.6 us -> 97.7 us
  Pallas kernels: 94.8 us -> 95.8 us
    pallas_call x1, Pallas kernels: 94.8 us -> 95.8 us  [on_device(): pl.pallas_call(layer_kernel, out_shape=jax.ShapeDtypeStruct((TOK, D), BF1...]
where the time goes in v4:
time: 97.9 us; the launch traced here: 97.7 us
  Pallas kernels  95.8 us (98%)
  local copies, waits for them, and re-layouts  1.88 us (2%)
    pallas_call x1, Pallas kernels, on_device(): pl.pallas_call(layer_kernel, out_shape=jax.ShapeDtypeStruct((TOK, D), BF1...  95.8 us

profile of v4, /device:TPU:1, one launch (start us, length us, event | category | flops | bytes accessed | tf_op | source)
XLA Modules:
  0.0 97.7 jit_solution(11312632694197277597)
XLA Ops:
  0.0 95.8 %layer.1 = bf16[128,2048]{1,0:T(8,128)(2,1)} custom-call(bf16[128,2048]{1,0:T(8,128)(2,1)} %bitcast.20, bf16[128,2048]{1,0:T(8,128)(2,1)} %bitcast.21, bf16[128,2048]{1,0:T(8,128)(2,1)} %bitcast.22, bf16[128,2048]{1,0:T(8,128)(2,1)} %bitcast.23, f32[16]{0:T(128)} %lam_ref.1, f32[16,128]{1,0:T(8,128)} %bitcast.24, f32[1,2048]{1,0:T(1,128)} %bitcast.25, ...), custom_call_target="tpu_custom_call" | custom-call | tf_op jit(solution)/shard_map/layer/pallas_call | solution.py:366
  95.8 1.9 %copy.15 = bf16[1,128,2048]{2,1,0:T(8,128)(2,1)} copy(bf16[1,128,2048]{2,1,0:T(8,128)(2,1)} %bitcast.19) | data formatting | bytes 1048576

commit v5 on v4

--- a/solution.py
+++ b/solution.py
@@ -17,7 +17,7 @@
 SLOTS = EXPERTS * CAP
 QB = 256
 STEPS = SEQ // QB
-HALF = STEPS // 2
+HALF = 6
 KC = 256
 RB = 16
 NC = 512
@@ -59,11 +59,11 @@
 def layer_kernel(
     q_hbm, k_hbm, v_hbm, res_hbm, lam_ref, gain_ref, ffn_ref, route_ref, weight_ref,
     wo_hbm, wg_hbm, wu_hbm, wd_hbm,
-    out_hbm,
+    out_ref,
     q_ref, k_ref, v_ref, res_ref,
-    qa, ka, va, s1a, s2a, s1b, s2b, maps, sums, obuf, att, total, mid, out, onehot, chigh, clow,
+    qa, ka, va, s1a, s2a, s1b, s2b, maps, sums, obuf, att, total, mid, onehot, chigh, clow,
     wo, wg, wu, wd, xs, rx, hid, yx, ret,
-    kvs, kvr, qs, qr, os_, or_, ds, dr, es, er, insem, wsem, outsem, ready,
+    kvs, kvr, qs, qr, os_, or_, ds, dr, es, er, insem, wsem, smallsem, ready,
 ):
     sp = lax.axis_index("sp")
     dp = lax.axis_index("dp")
@@ -233,7 +233,7 @@
             queries_arrive(step + 1)
             scores(step + 1, *later)
         mixed(step, *now)
-        for done in (2 * (step - HALF), 2 * (step - HALF) + 1):
+        for done in range((step - HALF) * STEPS // (STEPS - HALF), (step - HALF + 1) * STEPS // (STEPS - HALF)):
             valued(done)
             heads_leave(done)
 
@@ -286,9 +286,11 @@
 
     homes = [peer_of(sp, minus(off)) for off in PEERS] + [sp]
 
-    def batch(g, carry):
+    def arrive(g):
+        whole_batch(xs, rx, ds.at[g], dr.at[g], GROUP).wait_recv()
+
+    def work(g):
         at = rows_of(g, GROUP)
-        whole_batch(xs, rx, ds.at[g], dr.at[g], GROUP).wait_recv()
         x = rx[at].reshape(GROUP * CAP, D)
         for n in range(FF // 256):
             w = slice(n * 256, (n + 1) * 256)
@@ -300,6 +302,8 @@
             w = slice(n * NC, (n + 1) * NC)
             y = jnp.dot(h, wd[:, w], preferred_element_type=F32).astype(BF16)
             yx[at, :, w] = y.reshape(GROUP, CAP, NC)
+
+    def give_back(g):
         back_to = [[chip_core(dp, (8 - g - turn) % 4, dc) for dc in range(2)] for turn in range(4)]
         for j, (dz, dy, dc) in enumerate(INNER):
             i = g * GROUP + j
@@ -314,23 +318,36 @@
                 pl.when(g == OWN_GROUP)(own.start)
             else:
                 back.start()
+
+    def early(g, carry):
+        arrive(g)
+        work(g)
         return carry
 
-    lax.fori_loop(0, 4, batch, 0)
+    def late(g, carry):
+        give_back(g)
+        return carry
+
+    lax.fori_loop(0, 3, early, 0)
+    arrive(3)
+    lax.fori_loop(0, 3, late, 0)
+
+    def last(g, carry):
+        work(g)
+        give_back(g)
+        return carry
+
+    lax.fori_loop(3, 4, last, 0)
 
     for g in range(4):
         whole_batch(yx, ret, es.at[g], er.at[g], GROUP).wait_recv()
-    leaving = []
     for n in range(D // NC):
         at = slice(n * NC, (n + 1) * NC)
         r = ret[:, :, at].reshape(SLOTS, NC)
         dims = (((0,), (0,)), ((), ()))
         moe = lax.dot_general(chigh[...], r, dims, preferred_element_type=F32)
         moe = moe + lax.dot_general(clow[...], r, dims, preferred_element_type=F32)
-        out[:, at] = (mid[:, at].astype(F32) + moe).astype(BF16)
-        leave = pltpu.make_async_copy(out.at[:, at], out_hbm.at[:, at], outsem.at[n])
-        leave.start()
-        leaving.append(leave)
+        out_ref[:, at] = (mid[:, at].astype(F32) + moe).astype(BF16)
 
     all_blocks(ka, ka, kvs.at[0], kvr.at[0], 15).wait_send()
     all_blocks(va, va, kvs.at[1], kvr.at[1], 15).wait_send()
@@ -346,8 +363,6 @@
                 pl.when(to != sp)(copy.wait_send)
             else:
                 copy.wait_send()
-    for leave in leaving:
-        leave.wait()
 
 
 def on_device(
@@ -365,12 +380,12 @@
     sem = pltpu.SemaphoreType.DMA
     out = pl.pallas_call(
         layer_kernel,
-        out_shape=jax.ShapeDtypeStruct((TOK, D), BF16),
+        out_shape=pltpu.VMEM((TOK, D), BF16),
         in_specs=[hbm] * 4 + [smem] + [vmem] * 4 + [hbm] * 4,
-        out_specs=hbm,
+        out_specs=vmem,
         scratch_shapes=[tokens] * 4 + [rows, rows, rows, score, score, score, score,
                         pltpu.VMEM((STEPS, QB, SEQ), BF16), pltpu.VMEM((STEPS, QB, 1), F32), rows, tokens,
-                        pltpu.VMEM((TOK, D), F32), tokens, tokens,
+                        pltpu.VMEM((TOK, D), F32), tokens,
                         table, table, table,
                         pltpu.VMEM((D, D), BF16), pltpu.VMEM((D, FF), BF16),
                         pltpu.VMEM((D, FF), BF16), pltpu.VMEM((FF, D), BF16),

time: 97.9 us -> 96.1 us (0.982)
  local copies, waits for them, and re-layouts: 1.88 us -> 0.8 us
    unnamed x1, local copies, waits for them, and re-layouts: 1.88 us -> 0.8 us
where the time goes in v5:
time: 96.1 us; the launch traced here: 96 us
  Pallas kernels  95.1 us (99%)
    pallas_call x1, Pallas kernels, on_device(): pl.pallas_call(layer_kernel, out_shape=pltpu.VMEM((TOK, D), BF16), in_spe...  95.1 us

profile of v5, /device:TPU:1, one launch (start us, length us, event | category | flops | bytes accessed | tf_op | source)
XLA Modules:
  0.0 96.0 jit_solution(15502785785635520326)
XLA Ops:
  0.0 95.1 %layer.1 = bf16[128,2048]{1,0:T(8,128)(2,1)S(1)} custom-call(bf16[128,2048]{1,0:T(8,128)(2,1)} %bitcast.20, bf16[128,2048]{1,0:T(8,128)(2,1)} %bitcast.21, bf16[128,2048]{1,0:T(8,128)(2,1)} %bitcast.22, bf16[128,2048]{1,0:T(8,128)(2,1)} %bitcast.23, f32[16]{0:T(128)} %lam_ref.1, f32[16,128]{1,0:T(8,128)} %bitcast.24, f32[1,2048]{1,0:T(1,128)} %bitcast.25, ...), custom_call_target="tpu_custom_call" | custom-call | tf_op jit(solution)/shard_map/layer/pallas_call | solution.py:381
  95.2 0.8 copy.15

commit v6 on v5

--- a/solution.py
+++ b/solution.py
@@ -329,8 +329,9 @@
         return carry
 
     lax.fori_loop(0, 3, early, 0)
+    lax.fori_loop(0, 1, late, 0)
     arrive(3)
-    lax.fori_loop(0, 3, late, 0)
+    lax.fori_loop(1, 3, late, 0)
 
     def last(g, carry):
         work(g)

time: 96.1 us -> 95.9 us (level)
  no operation moved by 1% of the time
where the time goes in v6:
time: 95.9 us; the launch traced here: 95.8 us
  Pallas kernels  95 us (99%)
    pallas_call x1, Pallas kernels, on_device(): pl.pallas_call(layer_kernel, out_shape=pltpu.VMEM((TOK, D), BF16), in_spe...  95 us

profile of v6, /device:TPU:1, one launch (start us, length us, event | category | flops | bytes accessed | tf_op | source)
XLA Modules:
  0.0 95.8 jit_solution(14177485634010758394)
XLA Ops:
  0.0 95.0 %layer.1 = bf16[128,2048]{1,0:T(8,128)(2,1)S(1)} custom-call(bf16[128,2048]{1,0:T(8,128)(2,1)} %bitcast.20, bf16[128,2048]{1,0:T(8,128)(2,1)} %bitcast.21, bf16[128,2048]{1,0:T(8,128)(2,1)} %bitcast.22, bf16[128,2048]{1,0:T(8,128)(2,1)} %bitcast.23, f32[16]{0:T(128)} %lam_ref.1, f32[16,128]{1,0:T(8,128)} %bitcast.24, f32[1,2048]{1,0:T(1,128)} %bitcast.25, ...), custom_call_target="tpu_custom_call" | custom-call | tf_op jit(solution)/shard_map/layer/pallas_call | solution.py:382
  95.0 0.8 copy.15
